TPU v7x, 32 devices: a whole 2x2x4 slice. The times are simulated.
32 devices in a mesh: sp: 16 (over z, y, x), tp: 2 (over core).
Axes of the slice: x: 2, y: 2, z: 4, core: 2. Of those that a mesh axis runs over, the one named last changes fastest.
Arguments:
- residual: bfloat16 [2048, 4096], P('tp', 'sp'), may hold values from -6 to 6
- values: bfloat16 [4096, 4096], P('sp', 'tp'), may hold values from -6 to 6
- gate_input: bfloat16 [4096, 4096], P('sp', 'tp'), may hold values from -6 to 6
- group_keys: bfloat16 [4096, 3072], P('sp', 'tp'), may hold values from -6 to 6
- time_step: float32 [64, 4096], P('tp', 'sp'), may hold values from -8 to 14
- decay_rate: float32 [64], P('tp'), may hold values from 0 to 2
- skip_gain: float32 [64], P('tp'), may hold values from 0.25 to 2
- conv_values: bfloat16 [4, 4096], P(None, 'tp'), may hold values from -3 to 3
- conv_keys: bfloat16 [4, 3072], P(None, 'tp'), may hold values from -3 to 3
- mix_gain: float32 [4096], P('tp'), may hold values from 0.1 to 1.9
- out_weight: bfloat16 [4096, 2048], P('tp'), may hold values from -0.09375 to 0.09375
- norm_gain: float32 [2048], replicated, may hold values from 0.1 to 1.9
- hidden_gate: bfloat16 [2048, 5120], P('sp', 'tp'), may hold values from -0.125 to 0.125
- hidden_up: bfloat16 [2048, 5120], P('sp', 'tp'), may hold values from -0.125 to 0.125
- hidden_conv: bfloat16 [2, 3, 5120], P(None, None, 'tp'), may hold values from -3.5 to 3.5
- hidden_down: bfloat16 [5120, 2048], P('tp', 'sp'), may hold values from -0.078125 to 0.078125
Outputs:
- layer_out: bfloat16 [2048, 4096], P('tp', 'sp')
All inputs are finite; a program needn't handle non-finite values.
Results may differ from a plain program's by a relative error of at most 0.019.
Values may be sent and summed in bfloat16 or wider, within the bound.
A program may use at most 128 MiB of HBM per device.

v0:
```python
import functools

import jax
import jax.numpy as jnp
from jax import lax
from jax.experimental import pallas as pl
from jax.experimental.pallas import tpu as pltpu
from jax.sharding import PartitionSpec as P

GROUP_HEADS = 8
HEAD_SIZE = 64
STATE_WIDE = 128
STATE_NARROW = 64

NORM_FLOOR = 0.1
SPAN = 8
EDGE = 8
TILE = 16
LANES = 128
FIRST_BLOCKS = 1
SECOND_BLOCKS = 1
VMEM_LIMIT = 62 * 2**20
MESH = pl.DeviceIdType.MESH
HIGHEST = lax.Precision.HIGHEST


def flipped(place, turn, count):
    result = 0
    bit = 1
    while bit < count:
        own = (place // bit) % 2
        result = result + bit * (own + (turn // bit) % 2 * (1 - 2 * own))
        bit *= 2
    return result


def silu_taps(before, rows, taps):
    joined = jnp.concatenate([before.astype(jnp.float32), rows.astype(jnp.float32)], axis=0)
    count = rows.shape[0]
    first = before.shape[0] - taps.shape[0] + 1
    summed = taps[0:1].astype(jnp.float32) * joined[first : first + count]
    for tap in range(1, taps.shape[0]):
        summed = summed + taps[tap : tap + 1].astype(jnp.float32) * joined[
            first + tap : first + tap + count
        ]
    return summed * jax.nn.sigmoid(summed)


def causal_rows(value, count):
    row = lax.broadcasted_iota(jnp.int32, (count, count), 0)
    col = lax.broadcasted_iota(jnp.int32, (count, count), 1)
    return jnp.where(row >= col, value, -jnp.inf)


def token_mixer(
    sp_count, tp_count, span,
    values, keys, gates_far, time_step, decay_rate, skip, conv_values, conv_keys, mix_gain,
    weight_far, residual, both_far,
    merged, both_got,
    gates, weight, values_tail, keys_tail, run, delta, inputs, key_rows, local_out, gained,
    state, state_got, states_out, states_in, ends_own, ends, squares_own, squares_in,
    partial, partial_in,
    local_sems, tail_send, tail_recv, ends_send, ends_recv, state_send, state_recv,
    back_send, back_recv, square_send, square_recv, sum_send, sum_recv, both_send, both_recv,
):
    row_count = values.shape[0]
    head_count = time_step.shape[0]
    groups = head_count // GROUP_HEADS
    half = GROUP_HEADS // 2
    key_cols = 2 * STATE_WIDE + 2 * STATE_NARROW
    group_cols = GROUP_HEADS * HEAD_SIZE
    wide_rows = half * HEAD_SIZE
    narrow_rows = wide_rows * STATE_NARROW // STATE_WIDE
    group_rows = wide_rows + narrow_rows
    slice_rows = states_out.shape[1]
    owners = groups * group_rows // slice_rows
    rows = residual.shape[0]
    features = weight.shape[1]
    sp = lax.axis_index("sp")
    tp = lax.axis_index("tp")

    gate_copy = pltpu.make_async_copy(gates_far, gates, local_sems.at[0])
    gate_copy.start()
    weight_copy = pltpu.make_async_copy(weight_far, weight, local_sems.at[1])
    weight_copy.start()
    both_copy = pltpu.make_async_copy(both_far.at[sp % span], both_got.at[sp], local_sems.at[2])
    both_copy.start()

    others = [{"sp": flipped(sp, turn, sp_count)} for turn in range(1, sp_count)]
    siblings = [{"tp": (tp + step) % tp_count} for step in range(1, tp_count)]
    barrier = pltpu.get_barrier_semaphore()
    for peer in others + siblings:
        pl.semaphore_signal(barrier, inc=1, device_id=peer, device_id_type=MESH)

    deltas = jnp.maximum(time_step[...], 0.0) + jnp.log1p(jnp.exp(-jnp.abs(time_step[...])))
    delta[...] = deltas
    upto = lax.broadcasted_iota(jnp.int32, (row_count, row_count), 0) <= lax.broadcasted_iota(
        jnp.int32, (row_count, row_count), 1
    )
    running = jnp.dot(
        -decay_rate[...] * deltas, upto.astype(jnp.float32),
        precision=HIGHEST, preferred_element_type=jnp.float32,
    )
    run[...] = running
    tail_heads = jnp.concatenate(
        [running[:, row_count - LANES :], jnp.zeros((LANES - head_count, LANES), jnp.float32)], axis=0
    )
    last_rows = jnp.transpose(tail_heads)[LANES - 8 :, :]
    ends_own[...] = last_rows
    ends[sp] = last_rows

    pl.semaphore_wait(barrier, len(others) + len(siblings))

    started = []

    def go(copy):
        copy.start()
        started.append(copy)

    def remote(source, target, send, recv, peer):
        return pltpu.make_async_remote_copy(
            src_ref=source, dst_ref=target, send_sem=send, recv_sem=recv,
            device_id=peer, device_id_type=MESH,
        )

    after = {"sp": (sp + 1) % sp_count}
    last = slice(row_count - TILE, row_count)
    tails = [
        remote(values.at[last], values_tail, tail_send.at[0], tail_recv.at[0], after),
        remote(keys.at[last], keys_tail, tail_send.at[1], tail_recv.at[1], after),
    ]
    for copy in tails:
        go(copy)

    def both_block(turn):
        peer = flipped(sp, turn, sp_count)
        return remote(
            both_far.at[peer % span], both_got.at[sp], both_send.at[turn - 1], both_recv.at[turn - 1],
            {"sp": peer},
        )

    queue = list(range(sp_count - 1, 0, -1))

    def feed(count):
        for turn in queue[:count]:
            go(both_block(turn))
        del queue[:count]

    for turn in range(1, sp_count):
        peer = {"sp": flipped(sp, turn, sp_count)}
        go(remote(ends_own, ends.at[sp], ends_send.at[turn - 1], ends_recv.at[turn - 1], peer))
    feed(FIRST_BLOCKS)
    for copy in tails:
        copy.wait_recv()

    def heads_of(g):
        spot = pl.ds(pl.multiple_of(g * GROUP_HEADS, GROUP_HEADS), GROUP_HEADS)
        by_row = run[spot, :]
        return by_row, jnp.transpose(by_row), jnp.transpose(delta[spot, :])

    def value_cols(g):
        return pl.ds(pl.multiple_of(g * group_cols, LANES), group_cols)

    def keys_at(g, first, width):
        return key_rows[g, :, first : first + width]

    kinds = ((0, STATE_WIDE), (2 * STATE_WIDE, STATE_NARROW))

    def state_copy(owner, own_slice):
        return remote(
            state.at[own_slice], state_got.at[sp], state_send.at[owner], state_recv.at[sp], {"sp": owner}
        )

    def rows_of(owner):
        return pl.ds(pl.multiple_of(owner * slice_rows, 8), slice_rows)

    @pl.loop(0, groups)
    def _(g):
        cols = value_cols(g)
        key_span = pl.ds(pl.multiple_of(g * key_cols, LANES), key_cols)
        first = sp == 0
        before = jnp.where(first, 0.0, values_tail[TILE - 8 :, cols].astype(jnp.float32))
        inner = silu_taps(before, values[:, cols], conv_values[:, cols])
        inputs[:, cols] = inner
        before = jnp.where(first, 0.0, keys_tail[TILE - 8 :, key_span].astype(jnp.float32))
        made = silu_taps(before, keys[:, key_span], conv_keys[:, key_span]).astype(jnp.bfloat16)
        key_rows[g] = made
        by_row, by_col, deltas = heads_of(g)
        states = []
        for kind, (first_col, width) in enumerate(kinds):
            scaled = []
            for head in range(kind * half, (kind + 1) * half):
                own = slice(head * HEAD_SIZE, (head + 1) * HEAD_SIZE)
                to_end = jnp.exp(by_row[head : head + 1, row_count - 1 :] - by_col[:, head : head + 1])
                scaled.append((inner[:, own] * (deltas[:, head : head + 1] * to_end)).astype(jnp.bfloat16))
            states.append(
                lax.dot_general(
                    jnp.concatenate(scaled, axis=1),
                    made[:, first_col : first_col + width],
                    (((0,), (0,)), ((), ())),
                    preferred_element_type=jnp.float32,
                ).astype(jnp.bfloat16)
            )
        base = pl.multiple_of(g * group_rows, 8)
        state[pl.ds(base, wide_rows), :] = states[0]
        fold = STATE_WIDE // STATE_NARROW
        state[pl.ds(base + wide_rows, narrow_rows), :] = jnp.concatenate(
            [states[1][i * narrow_rows : (i + 1) * narrow_rows] for i in range(fold)], axis=1
        )
        per_group = group_rows // slice_rows

        @pl.loop(0, per_group)
        def _(index):
            owner = g * per_group + index

            @pl.when(owner != sp)
            def _():
                state_copy(owner, rows_of(owner)).start()

    feed(SECOND_BLOCKS)

    def inside(g):
        cols = value_cols(g)
        by_row, by_col, deltas = heads_of(g)
        inner = inputs[:, cols]
        outs = []
        for kind, (first_col, width) in enumerate(kinds):
            scores = lax.dot_general(
                keys_at(g, first_col + width, width), keys_at(g, first_col, width),
                (((1,), (1,)), ((), ())), preferred_element_type=jnp.float32,
            )
            for head in range(kind * half, (kind + 1) * half):
                own = slice(head * HEAD_SIZE, (head + 1) * HEAD_SIZE)
                gap = causal_rows(by_col[:, head : head + 1] - by_row[head : head + 1, :], row_count)
                mixing = (scores * jnp.exp(gap)).astype(jnp.bfloat16)
                weighted = (inner[:, own] * deltas[:, head : head + 1]).astype(jnp.bfloat16)
                outs.append(jnp.dot(mixing, weighted, preferred_element_type=jnp.float32))
        local_out[:, cols] = jnp.concatenate(outs, axis=1) + inner * skip[:, cols]

    ahead = (groups + 1) // 2
    @pl.loop(0, ahead)
    def _(g):
        inside(g)

    for turn in range(1, sp_count):
        peer = {"sp": flipped(sp, turn, sp_count)}
        remote(ends_own, ends.at[sp], ends_send.at[turn - 1], ends_recv.at[turn - 1], peer).wait_recv()

    def carry_all():
        for turn in range(1, sp_count):
            source = flipped(sp, turn, sp_count)
            remote(
                state.at[rows_of(sp)], state_got.at[source], state_send.at[sp], state_recv.at[source],
                {"sp": source},
            ).wait_recv()
        state_got[sp] = state[rows_of(sp), :]
        first_row = sp * slice_rows
        g = first_row // group_rows
        row = lax.broadcasted_iota(jnp.int32, (slice_rows, LANES), 0) + (first_row - g * group_rows)
        lane = lax.broadcasted_iota(jnp.int32, (slice_rows, LANES), 1)
        spans = ends[:, 7, :]
        shift = HEAD_SIZE.bit_length() - 1
        grown = []
        for side in range(STATE_WIDE // STATE_NARROW):
            wide_head = lax.shift_right_logical(row, shift)
            narrow_head = half + side * (narrow_rows // HEAD_SIZE) + lax.shift_right_logical(
                jnp.maximum(row - wide_rows, 0), shift
            )
            head = g * GROUP_HEADS + jnp.where(row < wide_rows, wide_head, narrow_head)
            grown.append(
                jnp.exp(
                    lax.dot_general(
                        (lane == head).astype(jnp.float32), spans, (((1,), (1,)), ((), ())),
                        precision=HIGHEST, preferred_element_type=jnp.float32,
                    )
                )
            )
        carry = jnp.zeros((slice_rows, LANES), jnp.float32)
        for source in range(sp_count):
            states_out[source] = carry.astype(jnp.bfloat16)
            factor = jnp.where(lane < STATE_NARROW, grown[0][:, source : source + 1], grown[1][:, source : source + 1])
            carry = carry * factor + state_got[source].astype(jnp.float32)
        states_in[rows_of(sp), :] = states_out[sp]
        for turn in range(1, sp_count):
            back_copy(sp, flipped(sp, turn, sp_count)).start()

    def back_copy(owner, target):
        return remote(
            states_out.at[target], states_in.at[rows_of(owner)], back_send.at[target], back_recv.at[owner],
            {"sp": target},
        )

    if owners < sp_count:
        pl.when(sp < owners)(carry_all)
    else:
        carry_all()
    feed(len(queue))

    @pl.loop(ahead, groups)
    def _(g):
        inside(g)

    gate_copy.wait()

    @pl.loop(0, owners)
    def _(owner):
        @pl.when(owner != sp)
        def _():
            back_copy(owner, sp).wait_recv()

    squares_own[...] = jnp.zeros(squares_own.shape, jnp.float32)

    @pl.loop(0, groups)
    def _(g):
        cols = value_cols(g)
        by_row, by_col, _ = heads_of(g)
        growth = jnp.exp(by_col)
        base = pl.multiple_of(g * group_rows, 8)
        wide_in = states_in[pl.ds(base, wide_rows), :]
        narrow_in = states_in[pl.ds(base + wide_rows, narrow_rows), :]
        reads = [
            lax.dot_general(
                keys_at(g, STATE_WIDE, STATE_WIDE), wide_in,
                (((1,), (1,)), ((), ())), preferred_element_type=jnp.float32,
            )
        ]
        for side in range(STATE_WIDE // STATE_NARROW):
            reads.append(
                lax.dot_general(
                    keys_at(g, 2 * STATE_WIDE + STATE_NARROW, STATE_NARROW),
                    narrow_in[:, side * STATE_NARROW : (side + 1) * STATE_NARROW],
                    (((1,), (1,)), ((), ())), preferred_element_type=jnp.float32,
                )
            )
        read = jnp.concatenate(reads, axis=1)
        parts = [
            read[:, head * HEAD_SIZE : (head + 1) * HEAD_SIZE] * growth[:, head : head + 1]
            for head in range(GROUP_HEADS)
        ]
        gate = gates[:, cols].astype(jnp.float32)
        gated = (local_out[:, cols] + jnp.concatenate(parts, axis=1)) * (gate * jax.nn.sigmoid(gate))
        power = gated * gated
        folded = power[:, :LANES]
        for first in range(LANES, group_cols, LANES):
            folded = folded + power[:, first : first + LANES]
        squares_own[...] += lax.dot_general(
            jnp.ones((8, LANES), jnp.float32), folded, (((1,), (1,)), ((), ())),
            precision=HIGHEST, preferred_element_type=jnp.float32,
        )
        gained[:, cols] = (gated * mix_gain[:, cols]).astype(jnp.bfloat16)

    for step in range(1, tp_count):
        go(remote(squares_own, squares_in.at[step - 1], square_send.at[step - 1], square_recv.at[step - 1], siblings[step - 1]))
    weight_copy.wait()
    wide_step = min(256, rows)

    @pl.loop(0, features // wide_step)
    def _(index):
        block = pl.ds(pl.multiple_of(index * wide_step, LANES), wide_step)
        product = jnp.dot(gained[...], weight[:, block], preferred_element_type=jnp.float32)
        partial[block, :] = jnp.transpose(product).astype(jnp.bfloat16)

    sums = []
    for step in range(1, tp_count):
        peer = pl.ds(pl.multiple_of((tp + step) % tp_count * rows, TILE), rows)
        copy = remote(
            partial.at[peer], partial_in.at[step - 1], sum_send.at[step - 1], sum_recv.at[step - 1], siblings[step - 1]
        )
        go(copy)
        sums.append(copy)
    square = squares_own[0:1, :]
    for step in range(1, tp_count):
        remote(squares_own, squares_in.at[step - 1], square_send.at[step - 1], square_recv.at[step - 1], siblings[step - 1]).wait_recv()
        square = square + squares_in[step - 1, 0:1, :]
    inverse = lax.rsqrt(square / (inputs.shape[1] * tp_count) + NORM_FLOOR)
    own_rows = pl.ds(pl.multiple_of(tp * rows, TILE), rows)
    summed = partial[own_rows, :].astype(jnp.float32)
    for step in range(1, tp_count):
        sums[step - 1].wait_recv()
        summed = summed + partial_in[step - 1].astype(jnp.float32)
    merged[...] = (residual[...].astype(jnp.float32) + summed * inverse).astype(jnp.bfloat16)

    for turn in range(1, sp_count):
        both_block(turn).wait_recv()
    both_copy.wait()
    for copy in started:
        copy.wait_send()

    @pl.loop(0, owners)
    def _(owner):
        @pl.when(owner != sp)
        def _():
            state_copy(owner, rows_of(owner)).wait_send()

    def back_done():
        for turn in range(1, sp_count):
            back_copy(sp, flipped(sp, turn, sp_count)).wait_send()

    if owners < sp_count:
        pl.when(sp < owners)(back_done)
    else:
        back_done()


def mixed_tokens(
    values, keys, gates, time_step, decay_rate, skip, conv_values, conv_keys, mix_gain,
    weight, residual, both, span,
):
    sp_count, tp_count = lax.axis_size("sp"), lax.axis_size("tp")
    row_count, inner = values.shape
    rows = residual.shape[0]
    head_count = time_step.shape[0]
    groups = head_count // GROUP_HEADS
    features = weight.shape[1]
    half_rows = GROUP_HEADS // 2 * HEAD_SIZE
    state_rows = groups * (half_rows + half_rows * STATE_NARROW // STATE_WIDE)
    slice_rows = max(8, state_rows // sp_count)
    owners = state_rows // slice_rows
    bf, f32 = jnp.bfloat16, jnp.float32
    dma = pltpu.SemaphoreType.DMA
    near = pl.BlockSpec(memory_space=pltpu.VMEM)
    far = pl.BlockSpec(memory_space=pltpu.MemorySpace.HBM)
    tp_others, others = tp_count - 1, sp_count - 1
    return pl.pallas_call(
        functools.partial(token_mixer, sp_count, tp_count, span),
        in_specs=[near, near, far, near, near, near, near, near, near, far, near, far],
        out_specs=[near, far],
        out_shape=[
            jax.ShapeDtypeStruct((rows, row_count), bf),
            jax.ShapeDtypeStruct((sp_count,) + both.shape[1:], bf),
        ],
        scratch_shapes=[
            pltpu.VMEM((row_count, inner), bf),
            pltpu.VMEM(weight.shape, bf),
            pltpu.VMEM((TILE, inner), bf),
            pltpu.VMEM((TILE, keys.shape[1]), bf),
            pltpu.VMEM((head_count, row_count), f32),
            pltpu.VMEM((head_count, row_count), f32),
            pltpu.VMEM((row_count, inner), f32),
            pltpu.VMEM((groups, row_count, keys.shape[1] // groups), bf),
            pltpu.VMEM((row_count, inner), f32),
            pltpu.VMEM((row_count, inner), bf),
            pltpu.VMEM((sp_count * slice_rows, LANES), bf),
            pltpu.VMEM((sp_count, slice_rows, LANES), bf),
            pltpu.VMEM((sp_count, slice_rows, LANES), bf),
            pltpu.VMEM((sp_count * slice_rows, LANES), bf),
            pltpu.VMEM((8, LANES), f32),
            pltpu.VMEM((sp_count, 8, LANES), f32),
            pltpu.VMEM((8, row_count), f32),
            pltpu.VMEM((tp_others, 8, row_count), f32),
            pltpu.VMEM((features, row_count), bf),
            pltpu.VMEM((tp_others, rows, row_count), bf),
            dma((3,)),
            dma((2,)),
            dma((2,)),
            dma((others,)),
            dma((others,)),
            dma((sp_count,)),
            dma((sp_count,)),
            dma((sp_count,)),
            dma((sp_count,)),
            dma((tp_others,)),
            dma((tp_others,)),
            dma((tp_others,)),
            dma((tp_others,)),
            dma((others,)),
            dma((others,)),
        ],
        compiler_params=pltpu.CompilerParams(
            collective_id=2, has_side_effects=True, vmem_limit_bytes=VMEM_LIMIT
        ),
        cost_estimate=pl.CostEstimate(flops=10**11, bytes_accessed=10**7, transcendentals=10**6),
        name="token_mixer",
    )(
        values, keys, gates, time_step, decay_rate, skip, conv_values, conv_keys, mix_gain,
        weight, residual, both,
    )


def row_parts(rows, count):
    bounds = [rows * part // count // TILE * TILE for part in range(count)] + [rows]
    return [slice(first, last) for first, last in zip(bounds[:-1], bounds[1:])]


def channel_mixer(
    sp_count, tp_count, span,
    merged, both_rows, down_blocks, gain, taps,
    out,
    wide, both_cols, down_rows, both_pre, edges, edge_out, edge_in, tap_wide, hidden,
    partial, tp_in, total, fold_a, fold_b, fold_c,
    own_sems, spread_send, spread_recv, side_send, side_recv, edge_send, edge_recv,
    sum_send, sum_recv, fold_send, fold_recv,
):
    rows, row_count = merged.shape
    width = both_cols.shape[0]
    quarter = width // 2
    features = both_cols.shape[1]
    sp = lax.axis_index("sp")
    tp = lax.axis_index("tp")
    place = sp % span
    base = sp - place
    own_rows = pl.ds(pl.multiple_of(tp * rows, TILE), rows)
    bits = [1 << i for i in range(span.bit_length() - 1)]
    turns = sorted(range(span), key=lambda turn: (turn.bit_count(), turn))
    slot = {turn: i for i, turn in enumerate(turns)}
    orders = [bits[i:] + bits[:i] for i in range(len(bits))]
    parts = row_parts(rows, len(bits))
    after = (sp + span) % sp_count
    behind = (sp + sp_count - span) % sp_count

    def member(turn):
        return {"sp": base + flipped(place, turn, span)}

    def sibling(step):
        return {"tp": (tp + step) % tp_count}

    barrier = pltpu.get_barrier_semaphore()
    greeted = [member(bit) for bit in bits] + [sibling(step) for step in range(1, tp_count)]
    if span < sp_count:
        greeted += [{"sp": after}, {"sp": behind}]
    for peer in greeted:
        pl.semaphore_signal(barrier, inc=1, device_id=peer, device_id_type=MESH)

    own_copy = pltpu.make_async_copy(merged, wide.at[0, own_rows], own_sems)
    own_copy.start()
    own_copy.wait()
    pl.semaphore_wait(barrier, len(greeted))

    def spread(part, bit, turn):
        place_rows = pl.ds(pl.multiple_of(tp * rows + parts[part].start, TILE), parts[part].stop - parts[part].start)
        index = slot[turn ^ bit] - 1
        return pltpu.make_async_remote_copy(
            src_ref=wide.at[slot[turn], place_rows],
            dst_ref=wide.at[slot[turn ^ bit], place_rows],
            send_sem=spread_send.at[part, index],
            recv_sem=spread_recv.at[part, index],
            device_id=member(bit),
            device_id_type=MESH,
        )

    def side(turn, step):
        return pltpu.make_async_remote_copy(
            src_ref=wide.at[slot[turn], own_rows],
            dst_ref=wide.at[slot[turn], own_rows],
            send_sem=side_send.at[slot[turn], step - 1],
            recv_sem=side_recv.at[slot[turn], step - 1],
            device_id=sibling(step),
            device_id_type=MESH,
        )

    started = []

    def go(copy):
        copy.start()
        started.append(copy)

    def arrived(part, turn):
        order = orders[part]
        last = [bit for bit in order if turn & bit][-1]
        spread(part, last, turn ^ last).wait_recv()

    def onward(part, turn):
        order = orders[part]
        reach = max([-1] + [i for i, bit in enumerate(order) if turn & bit])
        for bit in order[reach + 1 :]:
            go(spread(part, bit, turn))

    for position in range(len(bits)):
        for part in range(len(bits)):
            go(spread(part, orders[part][position], 0))

    def to_sides(turn):
        for step in range(1, tp_count):
            go(side(turn, step))

    def from_sides(turn):
        for step in range(1, tp_count):
            side(turn, step).wait_recv()

    to_sides(0)

    chunk = 128
    for first in range(0, features, chunk):
        cols = slice(first, first + chunk)
        block = jnp.transpose(both_rows[cols, :].astype(jnp.float32))
        both_cols[:, cols] = (block * gain[:, cols]).astype(jnp.bfloat16)
    count, _, narrow = down_blocks.shape

    @pl.loop(0, count)
    def _(index):
        block = jnp.transpose(down_blocks[index].astype(jnp.float32))
        down_rows[pl.ds(pl.multiple_of(index * narrow, narrow), narrow), :] = block.astype(jnp.bfloat16)

    for tap in range(taps.shape[1]):
        tap_wide[tap] = jnp.broadcast_to(taps[:, tap : tap + 1], (width, LANES))

    def project(index, turn):
        columns = wide[index]
        squares = jnp.zeros((8, row_count), jnp.float32)
        for first in range(0, features, 256):
            piece = columns[first : first + 256].astype(jnp.float32)
            squares = squares + jnp.sum((piece * piece).reshape(-1, 8, row_count), axis=0)
        mean = jnp.sum(squares, axis=0, keepdims=True) / features
        scale = lax.rsqrt(mean + NORM_FLOOR)
        pre = jnp.dot(both_cols[...], columns, preferred_element_type=jnp.float32) * scale
        both_pre[index] = pre.astype(jnp.bfloat16)
        edges[1 + flipped(place, turn, span)] = pre[:, row_count - LANES :].astype(jnp.bfloat16)

    from_sides(0)
    project(0, 0)
    events = []
    for part in range(len(bits)):
        for turn in turns[1:]:
            order = orders[part]
            key = [i for i, bit in enumerate(order) if turn & bit]
            events.append((max(key), len(key), key, part, turn))
    waiting = {turn: len(bits) for turn in turns[1:]}
    pending = []
    for _, _, _, part, turn in sorted(events):
        arrived(part, turn)
        onward(part, turn)
        waiting[turn] -= 1
        if waiting[turn] == 0:
            to_sides(turn)
            pending.append(turn)
            if len(pending) > 1:
                done = pending.pop(0)
                from_sides(done)
                project(slot[done], done)
    for done in pending:
        from_sides(done)
        project(slot[done], done)

    if span < sp_count:
        last = jnp.transpose(edges[span].astype(jnp.float32))
        edge_out[...] = last[LANES - TILE :, :].astype(jnp.bfloat16)
        edge_copy = pltpu.make_async_remote_copy(
            src_ref=edge_out, dst_ref=edge_in, send_sem=edge_send, recv_sem=edge_recv,
            device_id={"sp": after}, device_id_type=MESH,
        )
        edge_copy.start()
    edges[0] = jnp.zeros(edges.shape[1:], edges.dtype)

    lane = lax.broadcasted_iota(jnp.int32, (quarter, LANES), 1)

    def taps_of(index, spot):
        for first in range(0, row_count, LANES):
            sums = []
            for kind in range(2):
                own = slice(kind * quarter, (kind + 1) * quarter)
                now = both_pre[index, own, first : first + LANES].astype(jnp.float32)
                if first:
                    past = both_pre[index, own, first - LANES : first].astype(jnp.float32)
                else:
                    past = edges[spot, own, :].astype(jnp.float32)
                tap_count = taps.shape[1]
                summed = tap_wide[tap_count - 1, own, :] * now
                for back in range(1, tap_count):
                    moved = jnp.where(lane < back, pltpu.roll(past, back, 1), pltpu.roll(now, back, 1))
                    summed = summed + tap_wide[tap_count - 1 - back, own, :] * moved
                sums.append(summed)
            value = sums[0] * jax.nn.sigmoid(sums[0]) * sums[1]
            hidden[index, :, first : first + LANES] = value.astype(jnp.bfloat16)

    for turn in turns:
        taps_of(slot[turn], flipped(place, turn, span))
    if span < sp_count:
        edge_copy.wait()
        last = jnp.transpose(edge_in[...].astype(jnp.float32))
        own_edge = jnp.where(base == 0, 0.0, last)
        edges[0, :, LANES - TILE :] = own_edge.astype(jnp.bfloat16)
        for turn in turns:
            @pl.when(flipped(place, turn, span) == 0)
            def _():
                taps_of(slot[turn], 0)

    def to_sum(turn, step):
        peer = pl.ds(pl.multiple_of((tp + step) % tp_count * rows, TILE), rows)
        return pltpu.make_async_remote_copy(
            src_ref=partial.at[slot[turn], peer],
            dst_ref=tp_in.at[slot[turn], step - 1],
            send_sem=sum_send.at[slot[turn], step - 1],
            recv_sem=sum_recv.at[slot[turn], step - 1],
            device_id=sibling(step),
            device_id_type=MESH,
        )

    folds = (fold_a, fold_b, fold_c)

    def fold(part, stage, turn):
        bit = orders[part][stage]
        here = slot[turn ^ bit]
        return pltpu.make_async_remote_copy(
            src_ref=total.at[slot[turn], parts[part]],
            dst_ref=folds[stage].at[here, parts[part]],
            send_sem=fold_send.at[part, slot[turn] - 1],
            recv_sem=fold_recv.at[part, stage, here],
            device_id=member(bit),
            device_id_type=MESH,
        )

    def stage_of(part, turn):
        return min(i for i, bit in enumerate(orders[part]) if turn & bit)

    def multiply(turn):
        step_rows = min(512, features)
        for first in range(0, features, step_rows):
            block = slice(first, first + step_rows)
            partial[slot[turn], block] = jnp.dot(
                down_rows[block, :], hidden[slot[turn]], preferred_element_type=jnp.float32
            ).astype(jnp.bfloat16)
        for step in range(1, tp_count):
            go(to_sum(turn, step))

    def add_up(turn):
        summed = partial[slot[turn], own_rows].astype(jnp.float32)
        for step in range(1, tp_count):
            to_sum(turn, step).wait_recv()
            summed = summed + tp_in[slot[turn], step - 1].astype(jnp.float32)
        total[slot[turn]] = summed.astype(jnp.bfloat16)
        if turn:
            for part in range(len(bits)):
                if stage_of(part, turn) == 0:
                    go(fold(part, 0, turn))

    line = turns[::-1]
    for position, turn in enumerate(line):
        multiply(turn)
        if position:
            add_up(line[position - 1])
    add_up(line[-1])
    for stage in range(len(bits)):
        for part in range(len(bits)):
            order = orders[part]
            left = [turn for turn in turns if not any(turn & bit for bit in order[: stage + 1])]
            for turn in sorted(left, key=lambda turn: -turn.bit_count()):
                fold(part, stage, turn ^ order[stage]).wait_recv()
                summed = total[slot[turn], parts[part]].astype(jnp.float32) + folds[stage][
                    slot[turn], parts[part]
                ].astype(jnp.float32)
                if turn:
                    total[slot[turn], parts[part]] = summed.astype(jnp.bfloat16)
                    if stage_of(part, turn) == stage + 1:
                        go(fold(part, stage + 1, turn))
                elif stage + 1 < len(bits):
                    total[0, parts[part]] = summed.astype(jnp.bfloat16)
                else:
                    out[parts[part], :] = (merged[parts[part], :].astype(jnp.float32) + summed).astype(jnp.bfloat16)
    for copy in started:
        copy.wait_send()


def mixed_channels(merged, both_rows, down_blocks, gain, taps, span):
    rows, row_count = merged.shape
    sp_count, tp_count = lax.axis_size("sp"), lax.axis_size("tp")
    features, width = both_rows.shape
    quarter = width // 2
    levels = span.bit_length() - 1
    bf = jnp.bfloat16
    dma = pltpu.SemaphoreType.DMA
    vmem = pl.BlockSpec(memory_space=pltpu.VMEM)
    return pl.pallas_call(
        functools.partial(channel_mixer, sp_count, tp_count, span),
        in_specs=[vmem] * 5,
        out_specs=vmem,
        out_shape=jax.ShapeDtypeStruct((rows, row_count), bf),
        scratch_shapes=[
            pltpu.VMEM((span, features, row_count), bf),
            pltpu.VMEM((width, features), bf),
            pltpu.VMEM((features, quarter), bf),
            pltpu.VMEM((span, width, row_count), bf),
            pltpu.VMEM((span + 1, width, LANES), bf),
            pltpu.VMEM((TILE, width), bf),
            pltpu.VMEM((TILE, width), bf),
            pltpu.VMEM((taps.shape[1], width, LANES), jnp.float32),
            pltpu.VMEM((span, quarter, row_count), bf),
            pltpu.VMEM((span, features, row_count), bf),
            pltpu.VMEM((span, tp_count - 1, rows, row_count), bf),
            pltpu.VMEM((span, rows, row_count), bf),
            pltpu.VMEM((span, rows, row_count), bf),
            pltpu.VMEM((4, rows, row_count), bf),
            pltpu.VMEM((1, rows, row_count), bf),
            dma,
            dma((levels, span - 1)),
            dma((levels, span - 1)),
            dma((span, tp_count - 1)),
            dma((span, tp_count - 1)),
            dma,
            dma,
            dma((span, tp_count - 1)),
            dma((span, tp_count - 1)),
            dma((levels, span - 1)),
            dma((levels, levels, span)),
        ],
        compiler_params=pltpu.CompilerParams(
            collective_id=1, has_side_effects=True, vmem_limit_bytes=VMEM_LIMIT
        ),
        cost_estimate=pl.CostEstimate(flops=10**11, bytes_accessed=10**7, transcendentals=10**6),
        name="channel_mixer",
    )(merged, both_rows, down_blocks, gain, taps)


def local(
    residual,
    values,
    gate_input,
    group_keys,
    time_step,
    decay_rate,
    skip_gain,
    conv_values,
    conv_keys,
    mix_gain,
    out_weight,
    norm_gain,
    hidden_gate,
    hidden_up,
    hidden_conv,
    hidden_down,
):
    sp_count = lax.axis_size("sp")
    span = min(SPAN, sp_count)
    member = lax.axis_index("sp") % span
    rows, hidden_cols = hidden_gate.shape
    quarter = hidden_cols // span
    gates = hidden_gate.reshape(rows, span, quarter)
    ups = hidden_up.reshape(rows, span, quarter)
    both = jnp.transpose(jnp.concatenate([gates, ups], axis=2), (1, 0, 2))
    merged, both_rows = mixed_tokens(
        values, group_keys, gate_input, time_step, decay_rate[:, None],
        jnp.repeat(skip_gain, HEAD_SIZE)[None, :], conv_values, conv_keys, mix_gain[None, :],
        out_weight, residual, both, span,
    )
    down = hidden_down.reshape(span, quarter, hidden_down.shape[1])
    down = jnp.concatenate([down] * (sp_count // span), axis=0)
    down, merged = lax.optimization_barrier((down, merged))
    down_blocks = lax.all_to_all(down, "sp", 0, 0, tiled=True)
    own_taps = lax.dynamic_slice_in_dim(hidden_conv, member * quarter, quarter, 2)
    own_taps = jnp.transpose(own_taps, (0, 2, 1)).reshape(2 * quarter, -1).astype(jnp.float32)
    return mixed_channels(
        merged, both_rows.reshape(sp_count * rows, 2 * quarter), down_blocks, norm_gain[None, :], own_taps, span
    )


def solution(mesh):
    in_specs = (
        P("tp", "sp"),
        P("sp", "tp"),
        P("sp", "tp"),
        P("sp", "tp"),
        P("tp", "sp"),
        P("tp"),
        P("tp"),
        P(None, "tp"),
        P(None, "tp"),
        P("tp"),
        P("tp", None),
        P(),
        P("sp", "tp"),
        P("sp", "tp"),
        P(None, None, "tp"),
        P("tp", "sp"),
    )
    out_specs = P("tp", "sp")
    return jax.shard_map(local, mesh=mesh, in_specs=in_specs, out_specs=out_specs, check_vma=False)
```

profile of v0, /device:TPU:1, one launch (start us, length us, event | category | flops | bytes accessed | tf_op | source)
XLA Modules:
  0.0 214.4 jit_solution(16333324357859662204)
XLA Ops:
  0.0 0.0 copy-start.3
  0.0 0.0 copy-start.4
  0.0 0.0 copy-start.1
  0.0 2.5 %pad_maximum_fusion = bf16[16,320,128]{2,1,0:T(8,128)(2,1)} fusion(bf16[8,320,128]{2,1,0:T(8,128)(2,1)} %bitcast.14), kind=kLoop, calls=%fused_computation | loop fusion | flops 655360 | bytes 1966080 | tf_op jit(solution)/shard_map/concatenate | solution.py:835
  2.5 0.0 copy-done.3
  2.5 0.7 copy.23.decay_rate
  3.2 0.0 copy-done.4
  3.2 0.1 broadcast_in_dim.13
  3.3 0.7 broadcast_in_dim_reshape.3.skip
  4.0 0.0 copy-done.1
  4.0 0.0 copy-start.2
  4.0 0.3 copy.20
  4.3 0.4 copy.22
  4.7 0.4 copy-done.2
  5.1 0.3 copy.19
  5.4 0.4 copy.21
  5.8 1.5 maximum_bitcast_fusion.both_far
  7.3 87.3 %token_mixer.1 = (bf16[1024,256]{1,0:T(8,128)(2,1)}, bf16[16,128,640]{2,1,0:T(8,128)(2,1)}) custom-call(bf16[256,2048]{1,0:T(8,128)(2,1)} %values.1, bf16[256,1536]{1,0:T(8,128)(2,1)} %keys.1, bf16[256,2048]{1,0:T(8,128)(2,1)} %gates_far.1, f32[32,256]{1,0:T(8,128)} %time_step.1, f32[32,1]{1,0:T(8,128)} %copy.23.decay_rate, ...), custom_call_target="tpu_custom_call" | custom-call | flops 99999997952 | bytes 10000000 | tf_op jit(solution)/shard_map/token_mixer/pallas_call | solution.py:424
  94.6 6.0 %all-to-all-start = ((bf16[16,320,128]{2,1,0:T(8,128)(2,1)}), bf16[16,320,128]{2,1,0:T(8,128)(2,1)S(1)}, u32[]{:S(2)}, u32[]{:S(2)}) async-start(bf16[16,320,128]{2,1,0:T(8,128)(2,1)} %pad_maximum_fusion), calls=%async_computation | async-start | bytes 2621440 | tf_op jit(solution)/shard_map/all_to_all | solution.py:837
  100.6 0.8 convert_bitcast_fusion
  101.3 0.9 copy.24
  102.2 25.5 %all-to-all-done.down_blocks = bf16[16,320,128]{2,1,0:T(8,128)(2,1)S(1)} async-done(((bf16[16,320,128]{2,1,0:T(8,128)(2,1)}), bf16[16,320,128]{2,1,0:T(8,128)(2,1)S(1)}, u32[]{:S(2)}, u32[]{:S(2)}) %all-to-all-start) | async-done | bytes 1310752 | tf_op jit(solution)/shard_map/all_to_all | solution.py:837
  127.7 0.0 copy-start
  127.7 1.1 copy-done
  128.8 83.8 %channel_mixer.1 = bf16[1024,256]{1,0:T(8,128)(2,1)} custom-call(bf16[1024,256]{1,0:T(8,128)(2,1)} %get-tuple-element.10.merged, bf16[2048,640]{1,0:T(8,128)(2,1)} %bitcast.19, bf16[16,320,128]{2,1,0:T(8,128)(2,1)} %copy-done, f32[1,2048]{1,0:T(1,128)} %bitcast.18, f32[640,3]{1,0:T(8,128)} %bitcast.15), custom_call_target="tpu_custom_call" | custom-call | flops 99999997952 | bytes 10000000 | tf_op jit(solution)/shard_map/channel_mixer/pallas_call | solution.py:762
  212.6 1.9 copy.26
Async XLA Ops:
  0.0 2.5 %copy-start.3 = (f32[32]{0:T(128)S(1)}, f32[32]{0:T(128)}, u32[]{:S(2)}) copy-start(f32[32]{0:T(128)} %param.21) | copy-start | bytes 388
  0.0 3.2 %copy-start.4 = (f32[32]{0:T(128)S(1)}, f32[32]{0:T(128)}, u32[]{:S(2)}) copy-start(f32[32]{0:T(128)} %param.22) | copy-start | bytes 388
  0.0 4.0 %copy-start.1 = (bf16[128,2560]{1,0:T(8,128)(2,1)S(1)}, bf16[128,2560]{1,0:T(8,128)(2,1)}, u32[]{:S(2)}) copy-start(bf16[128,2560]{1,0:T(8,128)(2,1)} %param.29) | copy-start | bytes 1966084
  4.0 1.1 copy-start.2
  94.6 33.1 %all-to-all-start = ((bf16[16,320,128]{2,1,0:T(8,128)(2,1)}), bf16[16,320,128]{2,1,0:T(8,128)(2,1)S(1)}, u32[]{:S(2)}, u32[]{:S(2)}) async-start(bf16[16,320,128]{2,1,0:T(8,128)(2,1)} %pad_maximum_fusion), calls=%async_computation | async-start | bytes 2621440 | tf_op jit(solution)/shard_map/all_to_all | solution.py:837
  127.7 1.1 copy-start
where the time goes:
time: 216 us; the launch traced here: 214 us
  Pallas kernels  171 us (79%)
  waiting for transfers between devices  25.5 us (12%)
  local copies, waits for them, and re-layouts  7.04 us (3%)
  starting transfers between devices  5.97 us (3%)
  other arithmetic  4.78 us (2%)
    pallas_call x1, Pallas kernels, mixed_tokens(): pl.pallas_call(functools.partial(token_mixer, sp_count, tp_count, span),...  87.3 us
    pallas_call x1, Pallas kernels, mixed_channels(): pl.pallas_call(functools.partial(channel_mixer, sp_count, tp_count, span)...  83.8 us
    all_to_all x1, waiting for transfers between devices, local(): down_blocks = lax.all_to_all(down, 'sp', 0, 0, tiled=True)  25.5 us
    all_to_all x1, starting transfers between devices, local(): down_blocks = lax.all_to_all(down, 'sp', 0, 0, tiled=True)  5.97 us
  transfers between devices with their start and end apart: 1, of which 1 were waited for; matrix products, arithmetic and copies ran while one was open for 1% of the time, Pallas kernels for 0%

commit v1 on v0

--- a/solution.py
+++ b/solution.py
@@ -17,9 +17,9 @@
 EDGE = 8
 TILE = 16
 LANES = 128
-FIRST_BLOCKS = 1
-SECOND_BLOCKS = 1
-VMEM_LIMIT = 62 * 2**20
+FEEDS = ((1, 2), (1, 2), (1, 1), (0, 1), (0, 1), (1, 0))
+EVENT_FEEDS = {position: (1, 1) for position in range(3, 21)}
+VMEM_LIMIT = 63 * 2**20
 MESH = pl.DeviceIdType.MESH
 HIGHEST = lax.Precision.HIGHEST
 
@@ -52,17 +52,28 @@
     return jnp.where(row >= col, value, -jnp.inf)
 
 
-def token_mixer(
+def row_parts(rows, count):
+    bounds = [rows * part // count // TILE * TILE for part in range(count)] + [rows]
+    return [slice(first, last) for first, last in zip(bounds[:-1], bounds[1:])]
+
+
+def layer_kernel(
     sp_count, tp_count, span,
     values, keys, gates_far, time_step, decay_rate, skip, conv_values, conv_keys, mix_gain,
-    weight_far, residual, both_far,
-    merged, both_got,
-    gates, weight, values_tail, keys_tail, run, delta, inputs, key_rows, local_out, gained,
+    weight_far, residual, both_far, down_far, gain, taps,
+    out,
+    gates, slab, values_tail, keys_tail, run, delta, inputs, key_rows, local_out, gained,
     state, state_got, states_out, states_in, ends_own, ends, squares_own, squares_in,
-    partial, partial_in,
-    local_sems, tail_send, tail_recv, ends_send, ends_recv, state_send, state_recv,
-    back_send, back_recv, square_send, square_recv, sum_send, sum_recv, both_send, both_recv,
+    mixed, mixed_in, both_got, down_got,
+    wide, both_cols, down_rows, both_pre, edges, edge_out, edge_in, tap_wide, hidden,
+    tp_in, total, fold_a, fold_b, fold_c,
+    local_sems, weight_sems, tail_send, tail_recv, ends_send, ends_recv, state_send, state_recv,
+    back_send, back_recv, square_send, square_recv, mix_send, mix_recv, both_send, both_recv,
+    down_send, down_recv, spread_send, spread_recv, side_send, side_recv, edge_send, edge_recv,
+    sum_send, sum_recv, fold_send, fold_recv,
 ):
+    sp = lax.axis_index("sp")
+    tp = lax.axis_index("tp")
     row_count = values.shape[0]
     head_count = time_step.shape[0]
     groups = head_count // GROUP_HEADS
@@ -75,16 +86,26 @@
     slice_rows = states_out.shape[1]
     owners = groups * group_rows // slice_rows
     rows = residual.shape[0]
-    features = weight.shape[1]
-    sp = lax.axis_index("sp")
-    tp = lax.axis_index("tp")
+    features = wide.shape[1]
+    place = sp % span
+    base_place = sp - place
 
     gate_copy = pltpu.make_async_copy(gates_far, gates, local_sems.at[0])
     gate_copy.start()
-    weight_copy = pltpu.make_async_copy(weight_far, weight, local_sems.at[1])
-    weight_copy.start()
-    both_copy = pltpu.make_async_copy(both_far.at[sp % span], both_got.at[sp], local_sems.at[2])
+    weight_rows = weight_far.shape[0]
+    weight_copies = []
+    for index in range(features // row_count):
+        copy = pltpu.make_async_copy(
+            weight_far.at[:, index * row_count : (index + 1) * row_count],
+            slab.at[index, 0:weight_rows],
+            weight_sems.at[index],
+        )
+        copy.start()
+        weight_copies.append(copy)
+    both_copy = pltpu.make_async_copy(both_far.at[place], both_got.at[sp], local_sems.at[1])
     both_copy.start()
+    down_copy = pltpu.make_async_copy(down_far.at[place], down_got.at[sp], local_sems.at[2])
+    down_copy.start()
 
     others = [{"sp": flipped(sp, turn, sp_count)} for turn in range(1, sp_count)]
     siblings = [{"tp": (tp + step) % tp_count} for step in range(1, tp_count)]
@@ -139,17 +160,29 @@
             {"sp": peer},
         )
 
-    queue = list(range(sp_count - 1, 0, -1))
-
-    def feed(count):
-        for turn in queue[:count]:
-            go(both_block(turn))
-        del queue[:count]
+    def down_block(turn):
+        peer = flipped(sp, turn, sp_count)
+        return remote(
+            down_far.at[peer % span], down_got.at[sp], down_send.at[turn - 1], down_recv.at[turn - 1],
+            {"sp": peer},
+        )
+
+    far_turns = list(range(span, sp_count))
+    near_turns = list(range(1, span))
+    queue = [(both_block, far_turns), (both_block, near_turns), (down_block, far_turns), (down_block, near_turns)]
+    queue = [(kind, list(line)) for kind, line in queue]
+
+    def feed(far_count, near_count):
+        for first, count in ((0, far_count), (1, near_count)):
+            for _ in range(count):
+                kind, line = queue[first] if queue[first][1] else queue[first + 2]
+                if line:
+                    go(kind(line.pop(0)))
 
     for turn in range(1, sp_count):
         peer = {"sp": flipped(sp, turn, sp_count)}
         go(remote(ends_own, ends.at[sp], ends_send.at[turn - 1], ends_recv.at[turn - 1], peer))
-    feed(FIRST_BLOCKS)
+    feed(*FEEDS[0])
     for copy in tails:
         copy.wait_recv()
 
@@ -217,7 +250,7 @@
             def _():
                 state_copy(owner, rows_of(owner)).start()
 
-    feed(SECOND_BLOCKS)
+    feed(*FEEDS[1])
 
     def inside(g):
         cols = value_cols(g)
@@ -294,13 +327,14 @@
         pl.when(sp < owners)(carry_all)
     else:
         carry_all()
-    feed(len(queue))
+    feed(*FEEDS[2])
 
     @pl.loop(ahead, groups)
     def _(g):
         inside(g)
 
     gate_copy.wait()
+    feed(*FEEDS[3])
 
     @pl.loop(0, owners)
     def _(owner):
@@ -351,20 +385,17 @@
 
     for step in range(1, tp_count):
         go(remote(squares_own, squares_in.at[step - 1], square_send.at[step - 1], square_recv.at[step - 1], siblings[step - 1]))
-    weight_copy.wait()
-    wide_step = min(256, rows)
-
-    @pl.loop(0, features // wide_step)
-    def _(index):
-        block = pl.ds(pl.multiple_of(index * wide_step, LANES), wide_step)
-        product = jnp.dot(gained[...], weight[:, block], preferred_element_type=jnp.float32)
-        partial[block, :] = jnp.transpose(product).astype(jnp.bfloat16)
+    for index, copy in enumerate(weight_copies):
+        copy.wait()
+        product = jnp.dot(gained[...], slab[index, 0:weight_rows], preferred_element_type=jnp.float32)
+        mixed[index * row_count : (index + 1) * row_count, :] = jnp.transpose(product).astype(jnp.bfloat16)
+    feed(*FEEDS[4])
 
     sums = []
     for step in range(1, tp_count):
         peer = pl.ds(pl.multiple_of((tp + step) % tp_count * rows, TILE), rows)
         copy = remote(
-            partial.at[peer], partial_in.at[step - 1], sum_send.at[step - 1], sum_recv.at[step - 1], siblings[step - 1]
+            mixed.at[peer], mixed_in.at[step - 1], mix_send.at[step - 1], mix_recv.at[step - 1], siblings[step - 1]
         )
         go(copy)
         sums.append(copy)
@@ -374,160 +405,33 @@
         square = square + squares_in[step - 1, 0:1, :]
     inverse = lax.rsqrt(square / (inputs.shape[1] * tp_count) + NORM_FLOOR)
     own_rows = pl.ds(pl.multiple_of(tp * rows, TILE), rows)
-    summed = partial[own_rows, :].astype(jnp.float32)
+    summed = mixed[own_rows, :].astype(jnp.float32)
     for step in range(1, tp_count):
         sums[step - 1].wait_recv()
-        summed = summed + partial_in[step - 1].astype(jnp.float32)
-    merged[...] = (residual[...].astype(jnp.float32) + summed * inverse).astype(jnp.bfloat16)
-
-    for turn in range(1, sp_count):
-        both_block(turn).wait_recv()
-    both_copy.wait()
-    for copy in started:
-        copy.wait_send()
-
-    @pl.loop(0, owners)
-    def _(owner):
-        @pl.when(owner != sp)
-        def _():
-            state_copy(owner, rows_of(owner)).wait_send()
-
-    def back_done():
-        for turn in range(1, sp_count):
-            back_copy(sp, flipped(sp, turn, sp_count)).wait_send()
-
-    if owners < sp_count:
-        pl.when(sp < owners)(back_done)
-    else:
-        back_done()
-
-
-def mixed_tokens(
-    values, keys, gates, time_step, decay_rate, skip, conv_values, conv_keys, mix_gain,
-    weight, residual, both, span,
-):
-    sp_count, tp_count = lax.axis_size("sp"), lax.axis_size("tp")
-    row_count, inner = values.shape
-    rows = residual.shape[0]
-    head_count = time_step.shape[0]
-    groups = head_count // GROUP_HEADS
-    features = weight.shape[1]
-    half_rows = GROUP_HEADS // 2 * HEAD_SIZE
-    state_rows = groups * (half_rows + half_rows * STATE_NARROW // STATE_WIDE)
-    slice_rows = max(8, state_rows // sp_count)
-    owners = state_rows // slice_rows
-    bf, f32 = jnp.bfloat16, jnp.float32
-    dma = pltpu.SemaphoreType.DMA
-    near = pl.BlockSpec(memory_space=pltpu.VMEM)
-    far = pl.BlockSpec(memory_space=pltpu.MemorySpace.HBM)
-    tp_others, others = tp_count - 1, sp_count - 1
-    return pl.pallas_call(
-        functools.partial(token_mixer, sp_count, tp_count, span),
-        in_specs=[near, near, far, near, near, near, near, near, near, far, near, far],
-        out_specs=[near, far],
-        out_shape=[
-            jax.ShapeDtypeStruct((rows, row_count), bf),
-            jax.ShapeDtypeStruct((sp_count,) + both.shape[1:], bf),
-        ],
-        scratch_shapes=[
-            pltpu.VMEM((row_count, inner), bf),
-            pltpu.VMEM(weight.shape, bf),
-            pltpu.VMEM((TILE, inner), bf),
-            pltpu.VMEM((TILE, keys.shape[1]), bf),
-            pltpu.VMEM((head_count, row_count), f32),
-            pltpu.VMEM((head_count, row_count), f32),
-            pltpu.VMEM((row_count, inner), f32),
-            pltpu.VMEM((groups, row_count, keys.shape[1] // groups), bf),
-            pltpu.VMEM((row_count, inner), f32),
-            pltpu.VMEM((row_count, inner), bf),
-            pltpu.VMEM((sp_count * slice_rows, LANES), bf),
-            pltpu.VMEM((sp_count, slice_rows, LANES), bf),
-            pltpu.VMEM((sp_count, slice_rows, LANES), bf),
-            pltpu.VMEM((sp_count * slice_rows, LANES), bf),
-            pltpu.VMEM((8, LANES), f32),
-            pltpu.VMEM((sp_count, 8, LANES), f32),
-            pltpu.VMEM((8, row_count), f32),
-            pltpu.VMEM((tp_others, 8, row_count), f32),
-            pltpu.VMEM((features, row_count), bf),
-            pltpu.VMEM((tp_others, rows, row_count), bf),
-            dma((3,)),
-            dma((2,)),
-            dma((2,)),
-            dma((others,)),
-            dma((others,)),
-            dma((sp_count,)),
-            dma((sp_count,)),
-            dma((sp_count,)),
-            dma((sp_count,)),
-            dma((tp_others,)),
-            dma((tp_others,)),
-            dma((tp_others,)),
-            dma((tp_others,)),
-            dma((others,)),
-            dma((others,)),
-        ],
-        compiler_params=pltpu.CompilerParams(
-            collective_id=2, has_side_effects=True, vmem_limit_bytes=VMEM_LIMIT
-        ),
-        cost_estimate=pl.CostEstimate(flops=10**11, bytes_accessed=10**7, transcendentals=10**6),
-        name="token_mixer",
-    )(
-        values, keys, gates, time_step, decay_rate, skip, conv_values, conv_keys, mix_gain,
-        weight, residual, both,
-    )
-
-
-def row_parts(rows, count):
-    bounds = [rows * part // count // TILE * TILE for part in range(count)] + [rows]
-    return [slice(first, last) for first, last in zip(bounds[:-1], bounds[1:])]
-
-
-def channel_mixer(
-    sp_count, tp_count, span,
-    merged, both_rows, down_blocks, gain, taps,
-    out,
-    wide, both_cols, down_rows, both_pre, edges, edge_out, edge_in, tap_wide, hidden,
-    partial, tp_in, total, fold_a, fold_b, fold_c,
-    own_sems, spread_send, spread_recv, side_send, side_recv, edge_send, edge_recv,
-    sum_send, sum_recv, fold_send, fold_recv,
-):
-    rows, row_count = merged.shape
+        summed = summed + mixed_in[step - 1].astype(jnp.float32)
+    wide[0, own_rows] = (residual[...].astype(jnp.float32) + summed * inverse).astype(jnp.bfloat16)
+
     width = both_cols.shape[0]
     quarter = width // 2
-    features = both_cols.shape[1]
-    sp = lax.axis_index("sp")
-    tp = lax.axis_index("tp")
-    place = sp % span
-    base = sp - place
-    own_rows = pl.ds(pl.multiple_of(tp * rows, TILE), rows)
     bits = [1 << i for i in range(span.bit_length() - 1)]
     turns = sorted(range(span), key=lambda turn: (turn.bit_count(), turn))
     slot = {turn: i for i, turn in enumerate(turns)}
     orders = [bits[i:] + bits[:i] for i in range(len(bits))]
     parts = row_parts(rows, len(bits))
-    after = (sp + span) % sp_count
-    behind = (sp + sp_count - span) % sp_count
+    next_span = (sp + span) % sp_count
 
     def member(turn):
-        return {"sp": base + flipped(place, turn, span)}
+        return {"sp": base_place + flipped(place, turn, span)}
 
     def sibling(step):
-        return {"tp": (tp + step) % tp_count}
-
-    barrier = pltpu.get_barrier_semaphore()
-    greeted = [member(bit) for bit in bits] + [sibling(step) for step in range(1, tp_count)]
-    if span < sp_count:
-        greeted += [{"sp": after}, {"sp": behind}]
-    for peer in greeted:
-        pl.semaphore_signal(barrier, inc=1, device_id=peer, device_id_type=MESH)
-
-    own_copy = pltpu.make_async_copy(merged, wide.at[0, own_rows], own_sems)
-    own_copy.start()
-    own_copy.wait()
-    pl.semaphore_wait(barrier, len(greeted))
+        return siblings[step - 1]
+
+    def part_rows(part):
+        size = parts[part].stop - parts[part].start
+        return pl.ds(pl.multiple_of(tp * rows + parts[part].start, TILE), size)
 
     def spread(part, bit, turn):
-        place_rows = pl.ds(pl.multiple_of(tp * rows + parts[part].start, TILE), parts[part].stop - parts[part].start)
+        place_rows = part_rows(part)
         index = slot[turn ^ bit] - 1
         return pltpu.make_async_remote_copy(
             src_ref=wide.at[slot[turn], place_rows],
@@ -548,12 +452,6 @@
             device_id_type=MESH,
         )
 
-    started = []
-
-    def go(copy):
-        copy.start()
-        started.append(copy)
-
     def arrived(part, turn):
         order = orders[part]
         last = [bit for bit in order if turn & bit][-1]
@@ -578,18 +476,28 @@
             side(turn, step).wait_recv()
 
     to_sides(0)
-
-    chunk = 128
-    for first in range(0, features, chunk):
-        cols = slice(first, first + chunk)
-        block = jnp.transpose(both_rows[cols, :].astype(jnp.float32))
-        both_cols[:, cols] = (block * gain[:, cols]).astype(jnp.bfloat16)
-    count, _, narrow = down_blocks.shape
-
-    @pl.loop(0, count)
-    def _(index):
-        block = jnp.transpose(down_blocks[index].astype(jnp.float32))
-        down_rows[pl.ds(pl.multiple_of(index * narrow, narrow), narrow), :] = block.astype(jnp.bfloat16)
+    feed(*FEEDS[5])
+
+    def turn_both():
+        both_copy.wait()
+        for turn in range(1, sp_count):
+            both_block(turn).wait_recv()
+        chunk = 128
+        for first in range(0, features, chunk):
+            cols = slice(first, first + chunk)
+            each = both_got.shape[1]
+            block = both_got[first // each : (first + chunk) // each].reshape(chunk, width)
+            block = jnp.transpose(block.astype(jnp.float32))
+            both_cols[:, cols] = (block * gain[:, cols]).astype(jnp.bfloat16)
+
+    def turn_down():
+        down_copy.wait()
+        for turn in range(1, sp_count):
+            down_block(turn).wait_recv()
+        narrow = down_got.shape[2]
+        for index in range(sp_count):
+            block = jnp.transpose(down_got[index].astype(jnp.float32))
+            down_rows[index * narrow : (index + 1) * narrow, :] = block.astype(jnp.bfloat16)
 
     for tap in range(taps.shape[1]):
         tap_wide[tap] = jnp.broadcast_to(taps[:, tap : tap + 1], (width, LANES))
@@ -606,8 +514,6 @@
         both_pre[index] = pre.astype(jnp.bfloat16)
         edges[1 + flipped(place, turn, span)] = pre[:, row_count - LANES :].astype(jnp.bfloat16)
 
-    from_sides(0)
-    project(0, 0)
     events = []
     for part in range(len(bits)):
         for turn in turns[1:]:
@@ -615,28 +521,25 @@
             key = [i for i, bit in enumerate(order) if turn & bit]
             events.append((max(key), len(key), key, part, turn))
     waiting = {turn: len(bits) for turn in turns[1:]}
-    pending = []
-    for _, _, _, part, turn in sorted(events):
+    for position, (_, _, _, part, turn) in enumerate(sorted(events)):
         arrived(part, turn)
         onward(part, turn)
+        feed(*EVENT_FEEDS.get(position, (0, 0)))
         waiting[turn] -= 1
         if waiting[turn] == 0:
             to_sides(turn)
-            pending.append(turn)
-            if len(pending) > 1:
-                done = pending.pop(0)
-                from_sides(done)
-                project(slot[done], done)
-    for done in pending:
-        from_sides(done)
-        project(slot[done], done)
+    feed(2 * sp_count, 2 * sp_count)
+    turn_both()
+    for turn in turns:
+        from_sides(turn)
+        project(slot[turn], turn)
 
     if span < sp_count:
         last = jnp.transpose(edges[span].astype(jnp.float32))
         edge_out[...] = last[LANES - TILE :, :].astype(jnp.bfloat16)
         edge_copy = pltpu.make_async_remote_copy(
             src_ref=edge_out, dst_ref=edge_in, send_sem=edge_send, recv_sem=edge_recv,
-            device_id={"sp": after}, device_id_type=MESH,
+            device_id={"sp": next_span}, device_id_type=MESH,
         )
         edge_copy.start()
     edges[0] = jnp.zeros(edges.shape[1:], edges.dtype)
@@ -667,7 +570,7 @@
     if span < sp_count:
         edge_copy.wait()
         last = jnp.transpose(edge_in[...].astype(jnp.float32))
-        own_edge = jnp.where(base == 0, 0.0, last)
+        own_edge = jnp.where(base_place == 0, 0.0, last)
         edges[0, :, LANES - TILE :] = own_edge.astype(jnp.bfloat16)
         for turn in turns:
             @pl.when(flipped(place, turn, span) == 0)
@@ -677,7 +580,7 @@
     def to_sum(turn, step):
         peer = pl.ds(pl.multiple_of((tp + step) % tp_count * rows, TILE), rows)
         return pltpu.make_async_remote_copy(
-            src_ref=partial.at[slot[turn], peer],
+            src_ref=slab.at[slot[turn], peer],
             dst_ref=tp_in.at[slot[turn], step - 1],
             send_sem=sum_send.at[slot[turn], step - 1],
             recv_sem=sum_recv.at[slot[turn], step - 1],
@@ -706,14 +609,14 @@
         step_rows = min(512, features)
         for first in range(0, features, step_rows):
             block = slice(first, first + step_rows)
-            partial[slot[turn], block] = jnp.dot(
+            slab[slot[turn], block] = jnp.dot(
                 down_rows[block, :], hidden[slot[turn]], preferred_element_type=jnp.float32
             ).astype(jnp.bfloat16)
         for step in range(1, tp_count):
             go(to_sum(turn, step))
 
     def add_up(turn):
-        summed = partial[slot[turn], own_rows].astype(jnp.float32)
+        summed = slab[slot[turn], own_rows].astype(jnp.float32)
         for step in range(1, tp_count):
             to_sum(turn, step).wait_recv()
             summed = summed + tp_in[slot[turn], step - 1].astype(jnp.float32)
@@ -723,6 +626,7 @@
                 if stage_of(part, turn) == 0:
                     go(fold(part, 0, turn))
 
+    turn_down()
     line = turns[::-1]
     for position, turn in enumerate(line):
         multiply(turn)
@@ -745,59 +649,107 @@
                 elif stage + 1 < len(bits):
                     total[0, parts[part]] = summed.astype(jnp.bfloat16)
                 else:
-                    out[parts[part], :] = (merged[parts[part], :].astype(jnp.float32) + summed).astype(jnp.bfloat16)
+                    out[parts[part], :] = (wide[0, part_rows(part)].astype(jnp.float32) + summed).astype(jnp.bfloat16)
     for copy in started:
         copy.wait_send()
 
 
-def mixed_channels(merged, both_rows, down_blocks, gain, taps, span):
-    rows, row_count = merged.shape
+    @pl.loop(0, owners)
+    def _(owner):
+        @pl.when(owner != sp)
+        def _():
+            state_copy(owner, rows_of(owner)).wait_send()
+
+    def back_done():
+        for turn in range(1, sp_count):
+            back_copy(sp, flipped(sp, turn, sp_count)).wait_send()
+
+    if owners < sp_count:
+        pl.when(sp < owners)(back_done)
+    else:
+        back_done()
+
+
+def whole_layer(
+    values, keys, gates, time_step, decay_rate, skip, conv_values, conv_keys, mix_gain,
+    weight, residual, both, down, gain, taps, span,
+):
     sp_count, tp_count = lax.axis_size("sp"), lax.axis_size("tp")
-    features, width = both_rows.shape
+    row_count, inner = values.shape
+    rows = residual.shape[0]
+    head_count = time_step.shape[0]
+    groups = head_count // GROUP_HEADS
+    features = weight.shape[1]
+    half_rows = GROUP_HEADS // 2 * HEAD_SIZE
+    state_rows = groups * (half_rows + half_rows * STATE_NARROW // STATE_WIDE)
+    slice_rows = max(8, state_rows // sp_count)
+    width = both.shape[2]
     quarter = width // 2
     levels = span.bit_length() - 1
-    bf = jnp.bfloat16
-    dma = pltpu.SemaphoreType.DMA
-    vmem = pl.BlockSpec(memory_space=pltpu.VMEM)
+    bf, f32 = jnp.bfloat16, jnp.float32
+    near = pl.BlockSpec(memory_space=pltpu.VMEM)
+    far = pl.BlockSpec(memory_space=pltpu.MemorySpace.HBM)
+    tp_others, others = tp_count - 1, sp_count - 1
+    buffers = [
+        ((row_count, inner), bf),
+        ((max(span, features // row_count), features, row_count), bf),
+        ((TILE, inner), bf),
+        ((TILE, keys.shape[1]), bf),
+        ((head_count, row_count), f32),
+        ((head_count, row_count), f32),
+        ((row_count, inner), f32),
+        ((groups, row_count, keys.shape[1] // groups), bf),
+        ((row_count, inner), f32),
+        ((row_count, inner), bf),
+        ((sp_count * slice_rows, LANES), bf),
+        ((sp_count, slice_rows, LANES), bf),
+        ((sp_count, slice_rows, LANES), bf),
+        ((sp_count * slice_rows, LANES), bf),
+        ((8, LANES), f32),
+        ((sp_count, 8, LANES), f32),
+        ((8, row_count), f32),
+        ((tp_others, 8, row_count), f32),
+        ((features, row_count), bf),
+        ((tp_others, rows, row_count), bf),
+        ((sp_count,) + both.shape[1:], bf),
+        ((sp_count,) + down.shape[1:], bf),
+        ((span, features, row_count), bf),
+        ((width, features), bf),
+        ((features, quarter), bf),
+        ((span, width, row_count), bf),
+        ((span + 1, width, LANES), bf),
+        ((TILE, width), bf),
+        ((TILE, width), bf),
+        ((taps.shape[1], width, LANES), f32),
+        ((span, quarter, row_count), bf),
+        ((span, tp_others, rows, row_count), bf),
+        ((span, rows, row_count), bf),
+        ((span, rows, row_count), bf),
+        ((4, rows, row_count), bf),
+        ((1, rows, row_count), bf),
+    ]
+    counts = [
+        (3,), (features // row_count,), (2,), (2,), (others,), (others,), (sp_count,), (sp_count,),
+        (sp_count,), (sp_count,), (tp_others,), (tp_others,), (tp_others,), (tp_others,), (others,), (others,),
+        (others,), (others,), (levels, span - 1), (levels, span - 1), (span, tp_others), (span, tp_others), None, None,
+        (span, tp_others), (span, tp_others), (levels, span - 1), (levels, levels, span),
+    ]
     return pl.pallas_call(
-        functools.partial(channel_mixer, sp_count, tp_count, span),
-        in_specs=[vmem] * 5,
-        out_specs=vmem,
+        functools.partial(layer_kernel, sp_count, tp_count, span),
+        in_specs=[near, near, far, near, near, near, near, near, near, far, near, far, far, near, near],
+        out_specs=near,
         out_shape=jax.ShapeDtypeStruct((rows, row_count), bf),
-        scratch_shapes=[
-            pltpu.VMEM((span, features, row_count), bf),
-            pltpu.VMEM((width, features), bf),
-            pltpu.VMEM((features, quarter), bf),
-            pltpu.VMEM((span, width, row_count), bf),
-            pltpu.VMEM((span + 1, width, LANES), bf),
-            pltpu.VMEM((TILE, width), bf),
-            pltpu.VMEM((TILE, width), bf),
-            pltpu.VMEM((taps.shape[1], width, LANES), jnp.float32),
-            pltpu.VMEM((span, quarter, row_count), bf),
-            pltpu.VMEM((span, features, row_count), bf),
-            pltpu.VMEM((span, tp_count - 1, rows, row_count), bf),
-            pltpu.VMEM((span, rows, row_count), bf),
-            pltpu.VMEM((span, rows, row_count), bf),
-            pltpu.VMEM((4, rows, row_count), bf),
-            pltpu.VMEM((1, rows, row_count), bf),
-            dma,
-            dma((levels, span - 1)),
-            dma((levels, span - 1)),
-            dma((span, tp_count - 1)),
-            dma((span, tp_count - 1)),
-            dma,
-            dma,
-            dma((span, tp_count - 1)),
-            dma((span, tp_count - 1)),
-            dma((levels, span - 1)),
-            dma((levels, levels, span)),
-        ],
+        scratch_shapes=[pltpu.VMEM(shape, dtype) for shape, dtype in buffers]
+        + [pltpu.SemaphoreType.DMA(shape) if shape else pltpu.SemaphoreType.DMA for shape in counts],
         compiler_params=pltpu.CompilerParams(
             collective_id=1, has_side_effects=True, vmem_limit_bytes=VMEM_LIMIT
         ),
         cost_estimate=pl.CostEstimate(flops=10**11, bytes_accessed=10**7, transcendentals=10**6),
-        name="channel_mixer",
-    )(merged, both_rows, down_blocks, gain, taps)
+        name="layer_kernel",
+    )(
+        values, keys, gates, time_step, decay_rate, skip, conv_values, conv_keys, mix_gain,
+        weight, residual, both, down, gain, taps,
+    )
 
 
 def local(
@@ -826,19 +778,13 @@
     gates = hidden_gate.reshape(rows, span, quarter)
     ups = hidden_up.reshape(rows, span, quarter)
     both = jnp.transpose(jnp.concatenate([gates, ups], axis=2), (1, 0, 2))
-    merged, both_rows = mixed_tokens(
+    down = hidden_down.reshape(span, quarter, hidden_down.shape[1])
+    own_taps = lax.dynamic_slice_in_dim(hidden_conv, member * quarter, quarter, 2)
+    own_taps = jnp.transpose(own_taps, (0, 2, 1)).reshape(2 * quarter, -1).astype(jnp.float32)
+    return whole_layer(
         values, group_keys, gate_input, time_step, decay_rate[:, None],
         jnp.repeat(skip_gain, HEAD_SIZE)[None, :], conv_values, conv_keys, mix_gain[None, :],
-        out_weight, residual, both, span,
-    )
-    down = hidden_down.reshape(span, quarter, hidden_down.shape[1])
-    down = jnp.concatenate([down] * (sp_count // span), axis=0)
-    down, merged = lax.optimization_barrier((down, merged))
-    down_blocks = lax.all_to_all(down, "sp", 0, 0, tiled=True)
-    own_taps = lax.dynamic_slice_in_dim(hidden_conv, member * quarter, quarter, 2)
-    own_taps = jnp.transpose(own_taps, (0, 2, 1)).reshape(2 * quarter, -1).astype(jnp.float32)
-    return mixed_channels(
-        merged, both_rows.reshape(sp_count * rows, 2 * quarter), down_blocks, norm_gain[None, :], own_taps, span
+        out_weight, residual, both, down, norm_gain[None, :], own_taps, span,
     )
 
 

time: 216 us -> 184 us (0.85)
  waiting for transfers between devices: 25.5 us -> 0 us
  starting transfers between devices: 5.97 us -> 0 us
  other arithmetic: 4.78 us -> 2.28 us
    all_to_all x1 -> x0, waiting for transfers between devices: 25.5 us -> none  [local(): down_blocks = lax.all_to_all(down, 'sp', 0, 0, tiled=True)]
    all_to_all x1 -> x0, starting transfers between devices: 5.97 us -> none  [local(): down_blocks = lax.all_to_all(down, 'sp', 0, 0, tiled=True)]
    concatenate x1 -> x0, other arithmetic: 2.52 us -> none  [local(): down = jnp.concatenate([down] * (sp_count // span), axis=0)]
    pallas_call x2 -> x1, Pallas kernels: 171 us -> 172 us  [whole_layer(): pl.pallas_call(functools.partial(layer_kernel, sp_count, tp_count, span),...]
  transfers between devices with their start and end apart: 1 -> 0, of which waited for: 1 -> 0; matrix products, arithmetic and copies ran while one was open for 1% -> 0% of each run, Pallas kernels for 0% -> 0%
where the time goes in v1:
time: 184 us; the launch traced here: 182 us
  Pallas kernels  172 us (93%)
  local copies, waits for them, and re-layouts  8.03 us (4%)
  other arithmetic  2.28 us (1%)
    pallas_call x1, Pallas kernels, whole_layer(): pl.pallas_call(functools.partial(layer_kernel, sp_count, tp_count, span),...  172 us

profile of v1, /device:TPU:1, one launch (start us, length us, event | category | flops | bytes accessed | tf_op | source)
XLA Modules:
  0.0 182.2 jit_solution(1770863727529359320)
XLA Ops:
  0.0 0.0 copy-start
  0.0 1.4 copy.24.decay_rate
  1.4 0.7 broadcast_in_dim.13
  2.1 0.7 broadcast_in_dim_reshape.3.skip
  2.8 1.4 copy.20
  4.2 0.4 copy.22
  4.6 0.0 copy-done
  4.6 0.3 copy.19
  4.9 0.4 copy.21
  5.3 1.5 maximum_bitcast_fusion.both_far
  6.8 0.8 convert_bitcast_fusion
  7.6 0.9 copy.23
  8.5 171.8 %layer_kernel.1 = bf16[1024,256]{1,0:T(8,128)(2,1)} custom-call(bf16[256,2048]{1,0:T(8,128)(2,1)} %values.1, bf16[256,1536]{1,0:T(8,128)(2,1)} %keys.1, bf16[256,2048]{1,0:T(8,128)(2,1)} %gates_far.1, f32[32,256]{1,0:T(8,128)} %time_step.1, f32[32,1]{1,0:T(8,128)} %copy.24.decay_rate, f32[1,2048]{1,0:T(1,128)} %broadcast_in_dim_reshape.3.skip, ...), custom_call_target="tpu_custom_call" | custom-call | flops 99999997952 | bytes 10000000 | tf_op jit(solution)/shard_map/layer_kernel/pallas_call | solution.py:737
  180.3 1.9 %copy.26 = bf16[1024,256]{1,0:T(8,128)(2,1)} copy(bf16[1024,256]{1,0:T(8,128)(2,1)} %layer_kernel.1) | data formatting | bytes 1048576
Async XLA Ops:
  0.0 4.6 %copy-start = (bf16[128,2560]{1,0:T(8,128)(2,1)S(1)}, bf16[128,2560]{1,0:T(8,128)(2,1)}, u32[]{:S(2)}) copy-start(bf16[128,2560]{1,0:T(8,128)(2,1)} %param.28) | copy-start | bytes 1966084

commit v2 on v1

--- a/solution.py
+++ b/solution.py
@@ -16,8 +16,10 @@
 SPAN = 8
 EDGE = 8
 TILE = 16
+FAR_ORDER = (0, 2, 1, 2)
+SHARES = (5, 5, 5)
 LANES = 128
-FEEDS = ((1, 2), (1, 2), (1, 1), (0, 1), (0, 1), (1, 0))
+FEEDS = ((0, 3), (1, 2), (1, 2), (1, 0), (1, 0), (1, 0))
 EVENT_FEEDS = {position: (1, 1) for position in range(3, 21)}
 VMEM_LIMIT = 63 * 2**20
 MESH = pl.DeviceIdType.MESH
@@ -52,23 +54,25 @@
     return jnp.where(row >= col, value, -jnp.inf)
 
 
-def row_parts(rows, count):
-    bounds = [rows * part // count // TILE * TILE for part in range(count)] + [rows]
+def row_parts(rows, shares):
+    whole = sum(shares)
+    bounds = [rows * sum(shares[:part]) // whole // TILE * TILE for part in range(len(shares))] + [rows]
     return [slice(first, last) for first, last in zip(bounds[:-1], bounds[1:])]
 
 
 def layer_kernel(
     sp_count, tp_count, span,
-    values, keys, gates_far, time_step, decay_rate, skip, conv_values, conv_keys, mix_gain,
-    weight_far, residual, both_far, down_far, gain, taps,
+    values, keys, gates_far, time_step, decay_rate, skip_gain, conv_values, conv_keys, mix_gain,
+    weight_far, residual, gate_rows, up_rows, down_far, gain, taps,
     out,
-    gates, slab, values_tail, keys_tail, run, delta, inputs, key_rows, local_out, gained,
-    state, state_got, states_out, states_in, ends_own, ends, squares_own, squares_in,
+    both_far,
+    gates, slab, values_tail, keys_tail, run, delta, inputs, key_rows, gained,
+    state, state_got, states_out, states_in, state_sum, sums_got, ends_own, ends, squares_own, squares_in,
     mixed, mixed_in, both_got, down_got,
     wide, both_cols, down_rows, both_pre, edges, edge_out, edge_in, tap_wide, hidden,
     tp_in, total, fold_a, fold_b, fold_c,
     local_sems, weight_sems, tail_send, tail_recv, ends_send, ends_recv, state_send, state_recv,
-    back_send, back_recv, square_send, square_recv, mix_send, mix_recv, both_send, both_recv,
+    back_send, back_recv, total_send, total_recv, square_send, square_recv, mix_send, mix_recv, both_send, both_recv,
     down_send, down_recv, spread_send, spread_recv, side_send, side_recv, edge_send, edge_recv,
     sum_send, sum_recv, fold_send, fold_recv,
 ):
@@ -84,7 +88,9 @@
     narrow_rows = wide_rows * STATE_NARROW // STATE_WIDE
     group_rows = wide_rows + narrow_rows
     slice_rows = states_out.shape[1]
-    owners = groups * group_rows // slice_rows
+    owners = span
+    span_count = sp_count // span
+    group_of_spans = sp // span
     rows = residual.shape[0]
     features = wide.shape[1]
     place = sp % span
@@ -102,10 +108,15 @@
         )
         copy.start()
         weight_copies.append(copy)
-    both_copy = pltpu.make_async_copy(both_far.at[place], both_got.at[sp], local_sems.at[1])
-    both_copy.start()
     down_copy = pltpu.make_async_copy(down_far.at[place], down_got.at[sp], local_sems.at[2])
     down_copy.start()
+
+    quarter = gate_rows.shape[1] // span
+    for index in range(span):
+        cols = slice(index * quarter, (index + 1) * quarter)
+        both_far[index] = jnp.concatenate(
+            [gate_rows[:, cols].astype(jnp.float32), up_rows[:, cols].astype(jnp.float32)], axis=1
+        ).astype(jnp.bfloat16)
 
     others = [{"sp": flipped(sp, turn, sp_count)} for turn in range(1, sp_count)]
     siblings = [{"tp": (tp + step) % tp_count} for step in range(1, tp_count)]
@@ -118,8 +129,12 @@
     upto = lax.broadcasted_iota(jnp.int32, (row_count, row_count), 0) <= lax.broadcasted_iota(
         jnp.int32, (row_count, row_count), 1
     )
+    head_row = lax.broadcasted_iota(jnp.int32, (head_count, 1), 0)
+    rates = jnp.zeros((head_count, 1), jnp.float32)
+    for head in range(head_count):
+        rates = jnp.where(head_row == head, decay_rate[head], rates)
     running = jnp.dot(
-        -decay_rate[...] * deltas, upto.astype(jnp.float32),
+        -rates * deltas, upto.astype(jnp.float32),
         precision=HIGHEST, preferred_element_type=jnp.float32,
     )
     run[...] = running
@@ -167,7 +182,7 @@
             {"sp": peer},
         )
 
-    far_turns = list(range(span, sp_count))
+    far_turns = sorted(range(span, sp_count), key=lambda turn: (FAR_ORDER[turn % 4], turn))
     near_turns = list(range(1, span))
     queue = [(both_block, far_turns), (both_block, near_turns), (down_block, far_turns), (down_block, near_turns)]
     queue = [(kind, list(line)) for kind, line in queue]
@@ -199,9 +214,11 @@
 
     kinds = ((0, STATE_WIDE), (2 * STATE_WIDE, STATE_NARROW))
 
-    def state_copy(owner, own_slice):
+    def state_copy(owner, own_slice, source=None):
+        source = place if source is None else source
         return remote(
-            state.at[own_slice], state_got.at[sp], state_send.at[owner], state_recv.at[sp], {"sp": owner}
+            state.at[own_slice], state_got.at[source], state_send.at[owner], state_recv.at[source],
+            {"sp": base_place + owner},
         )
 
     def rows_of(owner):
@@ -246,7 +263,7 @@
         def _(index):
             owner = g * per_group + index
 
-            @pl.when(owner != sp)
+            @pl.when(owner != place)
             def _():
                 state_copy(owner, rows_of(owner)).start()
 
@@ -267,8 +284,11 @@
                 gap = causal_rows(by_col[:, head : head + 1] - by_row[head : head + 1, :], row_count)
                 mixing = (scores * jnp.exp(gap)).astype(jnp.bfloat16)
                 weighted = (inner[:, own] * deltas[:, head : head + 1]).astype(jnp.bfloat16)
-                outs.append(jnp.dot(mixing, weighted, preferred_element_type=jnp.float32))
-        local_out[:, cols] = jnp.concatenate(outs, axis=1) + inner * skip[:, cols]
+                outs.append(
+                    jnp.dot(mixing, weighted, preferred_element_type=jnp.float32)
+                    + inner[:, own] * skip_gain[g * GROUP_HEADS + head]
+                )
+        inputs[:, cols] = jnp.concatenate(outs, axis=1)
 
     ahead = (groups + 1) // 2
     @pl.loop(0, ahead)
@@ -279,19 +299,27 @@
         peer = {"sp": flipped(sp, turn, sp_count)}
         remote(ends_own, ends.at[sp], ends_send.at[turn - 1], ends_recv.at[turn - 1], peer).wait_recv()
 
+    def span_turn(turn):
+        peer = (sp + turn * span) % sp_count
+        return remote(
+            state_sum, sums_got.at[group_of_spans], total_send.at[turn], total_recv.at[group_of_spans],
+            {"sp": peer},
+        )
+
     def carry_all():
-        for turn in range(1, sp_count):
-            source = flipped(sp, turn, sp_count)
-            remote(
-                state.at[rows_of(sp)], state_got.at[source], state_send.at[sp], state_recv.at[source],
-                {"sp": source},
-            ).wait_recv()
-        state_got[sp] = state[rows_of(sp), :]
-        first_row = sp * slice_rows
+        for turn in range(1, span):
+            source = flipped(place, turn, span)
+            state_copy(place, rows_of(place), source).wait_recv()
+        state_got[place] = state[rows_of(place), :]
+        first_row = place * slice_rows
         g = first_row // group_rows
         row = lax.broadcasted_iota(jnp.int32, (slice_rows, LANES), 0) + (first_row - g * group_rows)
         lane = lax.broadcasted_iota(jnp.int32, (slice_rows, LANES), 1)
-        spans = ends[:, 7, :]
+        within = ends[pl.ds(base_place, span), 7, :]
+        each = [
+            jnp.sum(ends[i * span : (i + 1) * span, 7, :], axis=0, keepdims=True) for i in range(span_count)
+        ]
+        spans = jnp.concatenate([within] + each, axis=0)
         shift = HEAD_SIZE.bit_length() - 1
         grown = []
         for side in range(STATE_WIDE // STATE_NARROW):
@@ -308,25 +336,42 @@
                     )
                 )
             )
+
+        def factor(spot):
+            return jnp.where(lane < STATE_NARROW, grown[0][:, spot : spot + 1], grown[1][:, spot : spot + 1])
+
         carry = jnp.zeros((slice_rows, LANES), jnp.float32)
-        for source in range(sp_count):
+        if span_count > 1:
+            for source in range(span):
+                carry = carry * factor(source) + state_got[source].astype(jnp.float32)
+            state_sum[...] = carry.astype(jnp.bfloat16)
+            for turn in range(1, span_count):
+                go(span_turn(turn))
+            sums_got[group_of_spans] = jnp.zeros((slice_rows, LANES), jnp.bfloat16)
+            carry = jnp.zeros((slice_rows, LANES), jnp.float32)
+            for turn in range(1, span_count):
+                remote(
+                    state_sum, sums_got.at[(group_of_spans + turn) % span_count], total_send.at[turn],
+                    total_recv.at[(group_of_spans + turn) % span_count], {"sp": (sp + turn * span) % sp_count},
+                ).wait_recv()
+            for spot in range(span_count - 1):
+                further = carry * factor(span + spot) + sums_got[spot].astype(jnp.float32)
+                carry = jnp.where(spot < group_of_spans, further, carry)
+        for source in range(span):
             states_out[source] = carry.astype(jnp.bfloat16)
-            factor = jnp.where(lane < STATE_NARROW, grown[0][:, source : source + 1], grown[1][:, source : source + 1])
-            carry = carry * factor + state_got[source].astype(jnp.float32)
-        states_in[rows_of(sp), :] = states_out[sp]
-        for turn in range(1, sp_count):
-            back_copy(sp, flipped(sp, turn, sp_count)).start()
+            if source + 1 < span:
+                carry = carry * factor(source) + state_got[source].astype(jnp.float32)
+        states_in[rows_of(place), :] = states_out[place]
+        for turn in range(1, span):
+            back_copy(place, flipped(place, turn, span)).start()
 
     def back_copy(owner, target):
         return remote(
             states_out.at[target], states_in.at[rows_of(owner)], back_send.at[target], back_recv.at[owner],
-            {"sp": target},
-        )
-
-    if owners < sp_count:
-        pl.when(sp < owners)(carry_all)
-    else:
-        carry_all()
+            {"sp": base_place + target},
+        )
+
+    carry_all()
     feed(*FEEDS[2])
 
     @pl.loop(ahead, groups)
@@ -338,9 +383,9 @@
 
     @pl.loop(0, owners)
     def _(owner):
-        @pl.when(owner != sp)
+        @pl.when(owner != place)
         def _():
-            back_copy(owner, sp).wait_recv()
+            back_copy(owner, place).wait_recv()
 
     squares_own[...] = jnp.zeros(squares_own.shape, jnp.float32)
 
@@ -372,7 +417,7 @@
             for head in range(GROUP_HEADS)
         ]
         gate = gates[:, cols].astype(jnp.float32)
-        gated = (local_out[:, cols] + jnp.concatenate(parts, axis=1)) * (gate * jax.nn.sigmoid(gate))
+        gated = (inputs[:, cols] + jnp.concatenate(parts, axis=1)) * (gate * jax.nn.sigmoid(gate))
         power = gated * gated
         folded = power[:, :LANES]
         for first in range(LANES, group_cols, LANES):
@@ -417,7 +462,7 @@
     turns = sorted(range(span), key=lambda turn: (turn.bit_count(), turn))
     slot = {turn: i for i, turn in enumerate(turns)}
     orders = [bits[i:] + bits[:i] for i in range(len(bits))]
-    parts = row_parts(rows, len(bits))
+    parts = row_parts(rows, SHARES[: len(bits)])
     next_span = (sp + span) % sp_count
 
     def member(turn):
@@ -479,7 +524,7 @@
     feed(*FEEDS[5])
 
     def turn_both():
-        both_copy.wait()
+        both_got[sp] = both_far[place]
         for turn in range(1, sp_count):
             both_block(turn).wait_recv()
         chunk = 128
@@ -490,17 +535,30 @@
             block = jnp.transpose(block.astype(jnp.float32))
             both_cols[:, cols] = (block * gain[:, cols]).astype(jnp.bfloat16)
 
-    def turn_down():
-        down_copy.wait()
-        for turn in range(1, sp_count):
+    narrow = down_got.shape[2]
+    early = base_place * narrow // rows
+
+    def turn_down(first, waits):
+        for turn in waits:
             down_block(turn).wait_recv()
-        narrow = down_got.shape[2]
-        for index in range(sp_count):
-            block = jnp.transpose(down_got[index].astype(jnp.float32))
-            down_rows[index * narrow : (index + 1) * narrow, :] = block.astype(jnp.bfloat16)
-
-    for tap in range(taps.shape[1]):
-        tap_wide[tap] = jnp.broadcast_to(taps[:, tap : tap + 1], (width, LANES))
+        for index in range(span):
+            source = first + index
+            block = jnp.transpose(down_got[source].astype(jnp.float32))
+            down_rows[pl.ds(pl.multiple_of(source * narrow, narrow), narrow), :] = block.astype(jnp.bfloat16)
+
+    tap_total = taps.shape[1]
+    padded = (quarter + LANES - 1) // LANES * LANES
+    lines = jnp.concatenate(
+        [taps[0].astype(jnp.float32), taps[1].astype(jnp.float32), jnp.zeros((8 - 2 * tap_total, taps.shape[2]), jnp.float32)],
+        axis=0,
+    )
+    hidden_cols = taps.shape[2]
+    turned = pltpu.roll(lines, (hidden_cols - place * quarter) % hidden_cols, 1)
+    columns = jnp.transpose(turned[:, :padded])
+    for tap in range(tap_total):
+        for kind in range(2):
+            line = columns[:quarter, kind * tap_total + tap : kind * tap_total + tap + 1]
+            tap_wide[tap, kind * quarter : (kind + 1) * quarter] = jnp.broadcast_to(line, (quarter, LANES))
 
     def project(index, turn):
         columns = wide[index]
@@ -584,7 +642,7 @@
             dst_ref=tp_in.at[slot[turn], step - 1],
             send_sem=sum_send.at[slot[turn], step - 1],
             recv_sem=sum_recv.at[slot[turn], step - 1],
-            device_id=sibling(step),
+            device_id={"tp": (tp + step) % tp_count},
             device_id_type=MESH,
         )
 
@@ -605,15 +663,17 @@
     def stage_of(part, turn):
         return min(i for i, bit in enumerate(orders[part]) if turn & bit)
 
-    def multiply(turn):
-        step_rows = min(512, features)
-        for first in range(0, features, step_rows):
-            block = slice(first, first + step_rows)
+    def multiply(turn, owner):
+        step_rows = min(512, rows)
+        for first in range(0, rows, step_rows):
+            block = pl.ds(pl.multiple_of(owner * rows + first, step_rows), step_rows)
             slab[slot[turn], block] = jnp.dot(
                 down_rows[block, :], hidden[slot[turn]], preferred_element_type=jnp.float32
             ).astype(jnp.bfloat16)
-        for step in range(1, tp_count):
-            go(to_sum(turn, step))
+
+        @pl.when(owner != tp)
+        def _():
+            to_sum(turn, (owner + tp_count - tp) % tp_count).start()
 
     def add_up(turn):
         summed = slab[slot[turn], own_rows].astype(jnp.float32)
@@ -624,15 +684,31 @@
         if turn:
             for part in range(len(bits)):
                 if stage_of(part, turn) == 0:
-                    go(fold(part, 0, turn))
-
-    turn_down()
+                    fold(part, 0, turn).start()
+
     line = turns[::-1]
-    for position, turn in enumerate(line):
-        multiply(turn)
-        if position:
-            add_up(line[position - 1])
-    add_up(line[-1])
+    down_copy.wait()
+    turn_down(base_place, range(1, span))
+    for turn in line:
+        multiply(turn, early)
+
+    @pl.when(tp == early)
+    def _():
+        for turn in line:
+            add_up(turn)
+
+    for other in range(1, span_count):
+        waits = range(span, sp_count) if other == 1 else ()
+        turn_down((base_place + other * span) % sp_count, waits)
+    for turn in line:
+        for other in range(1, tp_count):
+            multiply(turn, (early + other) % tp_count)
+
+    @pl.when(tp != early)
+    def _():
+        for turn in line:
+            add_up(turn)
+
     for stage in range(len(bits)):
         for part in range(len(bits)):
             order = orders[part]
@@ -650,29 +726,29 @@
                     total[0, parts[part]] = summed.astype(jnp.bfloat16)
                 else:
                     out[parts[part], :] = (wide[0, part_rows(part)].astype(jnp.float32) + summed).astype(jnp.bfloat16)
+    for turn in turns:
+        for step in range(1, tp_count):
+            to_sum(turn, step).wait_send()
+        for part in range(len(bits)):
+            if turn and stage_of(part, turn) == 0:
+                fold(part, 0, turn).wait_send()
     for copy in started:
         copy.wait_send()
 
 
     @pl.loop(0, owners)
     def _(owner):
-        @pl.when(owner != sp)
+        @pl.when(owner != place)
         def _():
             state_copy(owner, rows_of(owner)).wait_send()
 
-    def back_done():
-        for turn in range(1, sp_count):
-            back_copy(sp, flipped(sp, turn, sp_count)).wait_send()
-
-    if owners < sp_count:
-        pl.when(sp < owners)(back_done)
-    else:
-        back_done()
+    for turn in range(1, span):
+        back_copy(place, flipped(place, turn, span)).wait_send()
 
 
 def whole_layer(
-    values, keys, gates, time_step, decay_rate, skip, conv_values, conv_keys, mix_gain,
-    weight, residual, both, down, gain, taps, span,
+    values, keys, gates, time_step, decay_rate, skip_gain, conv_values, conv_keys, mix_gain,
+    weight, residual, gate_rows, up_rows, down, gain, taps, span,
 ):
     sp_count, tp_count = lax.axis_size("sp"), lax.axis_size("tp")
     row_count, inner = values.shape
@@ -682,15 +758,18 @@
     features = weight.shape[1]
     half_rows = GROUP_HEADS // 2 * HEAD_SIZE
     state_rows = groups * (half_rows + half_rows * STATE_NARROW // STATE_WIDE)
-    slice_rows = max(8, state_rows // sp_count)
-    width = both.shape[2]
-    quarter = width // 2
+    slice_rows = state_rows // span
+    quarter = gate_rows.shape[1] // span
+    width = 2 * quarter
+    both_rows = gate_rows.shape[0]
     levels = span.bit_length() - 1
     bf, f32 = jnp.bfloat16, jnp.float32
     near = pl.BlockSpec(memory_space=pltpu.VMEM)
+    small = pl.BlockSpec(memory_space=pltpu.SMEM)
     far = pl.BlockSpec(memory_space=pltpu.MemorySpace.HBM)
     tp_others, others = tp_count - 1, sp_count - 1
     buffers = [
+        ((span, both_rows, width), bf),
         ((row_count, inner), bf),
         ((max(span, features // row_count), features, row_count), bf),
         ((TILE, inner), bf),
@@ -699,19 +778,20 @@
         ((head_count, row_count), f32),
         ((row_count, inner), f32),
         ((groups, row_count, keys.shape[1] // groups), bf),
-        ((row_count, inner), f32),
         ((row_count, inner), bf),
-        ((sp_count * slice_rows, LANES), bf),
-        ((sp_count, slice_rows, LANES), bf),
-        ((sp_count, slice_rows, LANES), bf),
-        ((sp_count * slice_rows, LANES), bf),
+        ((state_rows, LANES), bf),
+        ((span, slice_rows, LANES), bf),
+        ((span, slice_rows, LANES), bf),
+        ((state_rows, LANES), bf),
+        ((slice_rows, LANES), bf),
+        ((sp_count // span, slice_rows, LANES), bf),
         ((8, LANES), f32),
         ((sp_count, 8, LANES), f32),
         ((8, row_count), f32),
         ((tp_others, 8, row_count), f32),
         ((features, row_count), bf),
         ((tp_others, rows, row_count), bf),
-        ((sp_count,) + both.shape[1:], bf),
+        ((sp_count, both_rows, width), bf),
         ((sp_count,) + down.shape[1:], bf),
         ((span, features, row_count), bf),
         ((width, features), bf),
@@ -729,14 +809,14 @@
         ((1, rows, row_count), bf),
     ]
     counts = [
-        (3,), (features // row_count,), (2,), (2,), (others,), (others,), (sp_count,), (sp_count,),
-        (sp_count,), (sp_count,), (tp_others,), (tp_others,), (tp_others,), (tp_others,), (others,), (others,),
+        (3,), (features // row_count,), (2,), (2,), (others,), (others,), (span,), (span,),
+        (span,), (span,), (sp_count // span,), (sp_count // span,), (tp_others,), (tp_others,), (tp_others,), (tp_others,), (others,), (others,),
         (others,), (others,), (levels, span - 1), (levels, span - 1), (span, tp_others), (span, tp_others), None, None,
         (span, tp_others), (span, tp_others), (levels, span - 1), (levels, levels, span),
     ]
     return pl.pallas_call(
         functools.partial(layer_kernel, sp_count, tp_count, span),
-        in_specs=[near, near, far, near, near, near, near, near, near, far, near, far, far, near, near],
+        in_specs=[near, near, far, near, small, small, near, near, near, far, near, near, near, far, near, near],
         out_specs=near,
         out_shape=jax.ShapeDtypeStruct((rows, row_count), bf),
         scratch_shapes=[pltpu.VMEM(shape, dtype) for shape, dtype in buffers]
@@ -747,8 +827,8 @@
         cost_estimate=pl.CostEstimate(flops=10**11, bytes_accessed=10**7, transcendentals=10**6),
         name="layer_kernel",
     )(
-        values, keys, gates, time_step, decay_rate, skip, conv_values, conv_keys, mix_gain,
-        weight, residual, both, down, gain, taps,
+        values, keys, gates, time_step, decay_rate, skip_gain, conv_values, conv_keys, mix_gain,
+        weight, residual, gate_rows, up_rows, down, gain, taps,
     )
 
 
@@ -772,19 +852,11 @@
 ):
     sp_count = lax.axis_size("sp")
     span = min(SPAN, sp_count)
-    member = lax.axis_index("sp") % span
-    rows, hidden_cols = hidden_gate.shape
-    quarter = hidden_cols // span
-    gates = hidden_gate.reshape(rows, span, quarter)
-    ups = hidden_up.reshape(rows, span, quarter)
-    both = jnp.transpose(jnp.concatenate([gates, ups], axis=2), (1, 0, 2))
-    down = hidden_down.reshape(span, quarter, hidden_down.shape[1])
-    own_taps = lax.dynamic_slice_in_dim(hidden_conv, member * quarter, quarter, 2)
-    own_taps = jnp.transpose(own_taps, (0, 2, 1)).reshape(2 * quarter, -1).astype(jnp.float32)
+    down = hidden_down.reshape(span, hidden_gate.shape[1] // span, hidden_down.shape[1])
     return whole_layer(
-        values, group_keys, gate_input, time_step, decay_rate[:, None],
-        jnp.repeat(skip_gain, HEAD_SIZE)[None, :], conv_values, conv_keys, mix_gain[None, :],
-        out_weight, residual, both, down, norm_gain[None, :], own_taps, span,
+        values, group_keys, gate_input, time_step, decay_rate, skip_gain,
+        conv_values, conv_keys, mix_gain[None, :],
+        out_weight, residual, hidden_gate, hidden_up, down, norm_gain[None, :], hidden_conv, span,
     )
 
 

time: 184 us -> 172 us (0.935)
  local copies, waits for them, and re-layouts: 8.03 us -> 3.25 us
  Pallas kernels: 172 us -> 169 us
  other arithmetic: 2.28 us -> 0 us
    pallas_call x1, Pallas kernels: 172 us -> 169 us  [whole_layer(): pl.pallas_call(functools.partial(layer_kernel, sp_count, tp_count, span),...]
    broadcast_in_dim x2 -> x0, local copies, waits for them, and re-layouts: 2.12 us -> none  [the longest x1 1.4 us: local(): decay_rate[:, None]]
where the time goes in v2:
time: 172 us
  Pallas kernels  169 us (98%)
  local copies, waits for them, and re-layouts  3.25 us (2%)
    pallas_call x1, Pallas kernels, whole_layer(): pl.pallas_call(functools.partial(layer_kernel, sp_count, tp_count, span),...  169 us

profile of v2, /device:TPU:1, one launch (start us, length us, event | category | flops | bytes accessed | tf_op | source)
XLA Modules:
  0.0 171.8 jit_solution(15214142024963429961)
XLA Ops:
  0.0 1.4 copy.17.taps
  1.4 168.6 %layer_kernel.1 = bf16[1024,256]{1,0:T(8,128)(2,1)} custom-call(bf16[256,2048]{1,0:T(8,128)(2,1)} %values.1, bf16[256,1536]{1,0:T(8,128)(2,1)} %keys.1, bf16[256,2048]{1,0:T(8,128)(2,1)} %gates_far.1, f32[32,256]{1,0:T(8,128)} %time_step.1, f32[32]{0:T(128)} %decay_rate.1, f32[32]{0:T(128)} %skip_gain.1, bf16[4,2048]{1,0:T(4,128)(2,1)} %conv_values.1, ...), custom_call_target="tpu_custom_call" | custom-call | flops 99999997952 | bytes 10000000 | tf_op jit(solution)/shard_map/layer_kernel/pallas_call | solution.py:817
  170.0 1.9 %copy.19 = bf16[1024,256]{1,0:T(8,128)(2,1)} copy(bf16[1024,256]{1,0:T(8,128)(2,1)} %layer_kernel.1) | data formatting | bytes 1048576

commit v3 on v2

--- a/solution.py
+++ b/solution.py
@@ -689,25 +689,20 @@
     line = turns[::-1]
     down_copy.wait()
     turn_down(base_place, range(1, span))
-    for turn in line:
-        multiply(turn, early)
-
-    @pl.when(tp == early)
-    def _():
-        for turn in line:
-            add_up(turn)
+    def pipelined(chosen, owners_of):
+        for position, turn in enumerate(line + [None]):
+            if turn is not None:
+                for owner in owners_of:
+                    multiply(turn, owner)
+            if position:
+                pl.when(chosen)(functools.partial(add_up, line[position - 1]))
+
+    pipelined(tp == early, [early])
 
     for other in range(1, span_count):
         waits = range(span, sp_count) if other == 1 else ()
         turn_down((base_place + other * span) % sp_count, waits)
-    for turn in line:
-        for other in range(1, tp_count):
-            multiply(turn, (early + other) % tp_count)
-
-    @pl.when(tp != early)
-    def _():
-        for turn in line:
-            add_up(turn)
+    pipelined(tp != early, [(early + other) % tp_count for other in range(1, tp_count)])
 
     for stage in range(len(bits)):
         for part in range(len(bits)):

time: 172 us -> 170 us (0.988)
  Pallas kernels: 169 us -> 166 us
    pallas_call x1, Pallas kernels: 169 us -> 166 us  [whole_layer(): pl.pallas_call(functools.partial(layer_kernel, sp_count, tp_count, span),...]
where the time goes in v3:
time: 170 us
  Pallas kernels  166 us (98%)
  local copies, waits for them, and re-layouts  3.25 us (2%)
    pallas_call x1, Pallas kernels, whole_layer(): pl.pallas_call(functools.partial(layer_kernel, sp_count, tp_count, span),...  166 us

profile of v3, /device:TPU:1, one launch (start us, length us, event | category | flops | bytes accessed | tf_op | source)
XLA Modules:
  0.0 169.6 jit_solution(6248869741356858058)
XLA Ops:
  0.0 1.4 copy.17.taps
  1.4 166.4 %layer_kernel.1 = bf16[1024,256]{1,0:T(8,128)(2,1)} custom-call(bf16[256,2048]{1,0:T(8,128)(2,1)} %values.1, bf16[256,1536]{1,0:T(8,128)(2,1)} %keys.1, bf16[256,2048]{1,0:T(8,128)(2,1)} %gates_far.1, f32[32,256]{1,0:T(8,128)} %time_step.1, f32[32]{0:T(128)} %decay_rate.1, f32[32]{0:T(128)} %skip_gain.1, bf16[4,2048]{1,0:T(4,128)(2,1)} %conv_values.1, ...), custom_call_target="tpu_custom_call" | custom-call | flops 99999997952 | bytes 10000000 | tf_op jit(solution)/shard_map/layer_kernel/pallas_call | solution.py:812
  167.8 1.9 %copy.19 = bf16[1024,256]{1,0:T(8,128)(2,1)} copy(bf16[1024,256]{1,0:T(8,128)(2,1)} %layer_kernel.1) | data formatting | bytes 1048576
